TPU v7x, 512 devices: a whole 4x8x8 slice. The times are simulated.
512 devices in a mesh: fs: 64 (over z, y), tp: 8 (over x, core).
Axes of the slice: x: 4, y: 8, z: 8, core: 2. Of those that a mesh axis runs over, the one named last changes fastest.
Arguments:
- inputs: bfloat16 [24576, 2048], P('fs'), may hold values from -6 to 6
- gain: float32 [2048], replicated, may hold values from 0.1 to 1.9
- w_gate: bfloat16 [2048, 2816], P('fs', 'tp'), may hold values from -0.125 to 0.125
- w_up: bfloat16 [2048, 2816], P('fs', 'tp'), may hold values from -0.125 to 0.125
- w_down: bfloat16 [2816, 2048], P('tp', 'fs'), may hold values from -0.109375 to 0.109375
- cotangent: bfloat16 [24576, 2048], P('fs'), may hold values from -16 to 16
Outputs:
- input_gradient: bfloat16 [24576, 2048], P('fs')
- grad_down: float32 [2816, 2048], P('tp', 'fs')
All inputs are finite; a program needn't handle non-finite values.
Results may differ from a plain program's by a relative error of at most 0.014.
Values may be sent and summed in bfloat16 or wider, within the bound.
No kernel may reach another device: no remote copies, remote signals or barrier semaphores. Data moves between devices by JAX's collectives and lax.ppermute only.
A program may use at most 64 MiB of HBM per device.

v0:
```python
import jax
import jax.numpy as jnp
from jax import lax
from jax.experimental import pallas as pl
from jax.experimental.pallas import tpu as pltpu
from jax.sharding import Mesh
from jax.sharding import PartitionSpec as P


AXES = ("z", "y", "x", "c")
NZ, NY, NX, NC = 8, 8, 4, 2
FS = ("z", "y")
TP = ("x", "c")
EPSILON = 1e-06
HALF_STEP = 0.5
TOK = 384
D = 2048
HU = 352
HP = 384
DROWS = 32
HALF = TOK // NC
QUARTER = HALF // NX
VMEM_LIMIT = 28 * 2**20
SMALL_LIMIT = 6 * 2**20
DOWN_LIMIT = 16 * 2**20


def device_number(z, y, x, c):
    return ((z % NZ * NY + y % NY) * NX + x) * NC + c


def ring_pairs(step):
    return [
        (device_number(z, y, x, c), device_number(z + (1 - c) * step, y + c * step, x, c))
        for z in range(NZ)
        for y in range(NY)
        for x in range(NX)
        for c in range(NC)
    ]


def line_groups(along_ring):
    groups = []
    for x in range(NX):
        for c in range(NC):
            vary_z = (c == 0) == along_ring
            for fixed in range(8):
                groups.append(
                    [
                        device_number(k, fixed, x, c) if vary_z else device_number(fixed, k, x, c)
                        for k in range(8)
                    ]
                )
    return groups


def ring(array, step):
    return lax.ppermute(array, AXES, ring_pairs(step))


def exchange(array, along_ring):
    return lax.all_to_all(
        array, AXES, 0, 0, axis_index_groups=line_groups(along_ring), tiled=True
    )


def dot(left, right, dims):
    return lax.dot_general(left, right, (dims, ((), ())), preferred_element_type=jnp.float32)


def half_rows(core):
    return pl.ds(pl.multiple_of(core * HALF, 64), HALF)


def normalize_kernel(x_ref, gain_ref, xn_ref, half_ref):
    half_ref[...] = x_ref[half_rows(lax.axis_index("c")), :]
    gain = gain_ref[...]
    for k in range(6):
        rows = pl.ds(k * 64, 64)
        value = x_ref[rows, :].astype(jnp.float32)
        inverse = lax.rsqrt(jnp.mean(value * value, axis=-1, keepdims=True) + EPSILON)
        xn_ref[rows, :] = (value * inverse * gain).astype(jnp.bfloat16)


def block_rows(q, o):
    q = lax.rem(q + 16, 8)
    c = lax.axis_index("c")
    return pl.ds(pl.multiple_of(jnp.where(c == 0, q * 256 + o * 32, o * 256 + q * 32), 32), DROWS)


def ring_place():
    return jnp.where(lax.axis_index("c") == 0, lax.axis_index("z"), lax.axis_index("y"))


def early_kernel(
    norm_ref, cot_ref, b0, p1, p2, p3, m1, m2, m3, w_ref, gate_up_ref, d_hidden_ref
):
    r = ring_place()
    places = (r, r - 1, r - 2, r - 3, r + 1, r + 2, r + 3)
    for q, block in zip(places, (b0, p1, p2, p3, m1, m2, m3)):
        for o in range(8):
            w_ref[block_rows(q, o), :] = block[pl.ds(o * DROWS, DROWS), :]
    for o in range(8):
        w_ref[block_rows(r + 4, o), :] = jnp.zeros((DROWS, 3 * HP), jnp.bfloat16)
    gate_up_ref[...] = dot(norm_ref[...], w_ref[:, : 2 * HP], ((1,), (0,)))
    d_hidden_ref[...] = dot(cot_ref[...], w_ref[:, 2 * HP :], ((1,), (0,)))


def compute_kernel(
    w_in, gate_up_ref, d_hidden_ref, turned_x, turned_cot, p4, m4,
    keep_ref, send_ref, hidden_ref, w_ref, part_ref, last_ref,
):
    c = lax.axis_index("c")
    r = ring_place()
    last_ref[pl.ds(0, 128), :] = p4[...]
    last_ref[pl.ds(128, 128), :] = m4[...]
    for o in range(8):
        w_ref[block_rows(r + 4, o), :] = last_ref[pl.ds(o * DROWS, DROWS), :]

    last = pl.ds(pl.multiple_of(lax.rem(r + 4, 8) * 256, 256), 256)
    gate_up = gate_up_ref[...] + dot(turned_x[...], last_ref[:, : 2 * HP], ((0,), (0,)))
    gate = gate_up[:, :HP]
    up = gate_up[:, HP:]
    d_hidden = d_hidden_ref[...] + dot(turned_cot[last, :], last_ref[:, 2 * HP :], ((0,), (0,)))
    d_hidden = HALF_STEP * d_hidden
    sig = jax.nn.sigmoid(gate)
    hidden = (gate * sig * up).astype(jnp.bfloat16)
    d_gate = (d_hidden * up * sig * (1.0 + gate * (1.0 - sig))).astype(jnp.bfloat16)
    d_up = (d_hidden * gate * sig).astype(jnp.bfloat16)
    both = jnp.concatenate([d_gate, d_up], axis=1)
    part_ref[...] = dot(both, w_ref[:, : 2 * HP], ((1,), (1,))).astype(jnp.bfloat16)
    hidden_ref[...] = hidden
    keep_ref[...] = part_ref[half_rows(c), :]
    send_ref[...] = part_ref[half_rows(1 - c), :]


def turn_into(source_ref, turned_ref):
    c = lax.axis_index("c")
    for z in range(NZ):
        block = source_ref[:, z * 256 : (z + 1) * 256].T
        for y in range(NY):
            row = jnp.where(c == 0, z * 256 + y * 32, y * 256 + z * 32)
            rows = pl.ds(pl.multiple_of(row, 32), DROWS)
            turned_ref[rows, :] = block[y * 32 : (y + 1) * 32, :]


def turn_kernel(cot_ref, norm_ref, turned_ref, last_x_ref, all_ref):
    turn_into(cot_ref, turned_ref)
    turn_into(norm_ref, all_ref)
    last = pl.multiple_of(lax.rem(ring_place() + 4, 8) * 256, 256)
    last_x_ref[...] = all_ref[pl.ds(last, 256), :]


def down_kernel(turned_ref, hidden_ref, down_ref, staged_ref, sems):
    hidden = hidden_ref[...]
    copies = []
    for q in range(8):
        block = pl.ds(q * 256, 256)
        down = HALF_STEP * dot(turned_ref[block, :], hidden, ((1,), (0,)))
        staged_ref[block, :] = down.astype(jnp.bfloat16)
        copies.append(
            pltpu.make_async_copy(staged_ref.at[block, :], down_ref.at[block, :], sems.at[q])
        )
        copies[-1].start()
    for copy in copies:
        copy.wait()


def vmem_specs(count):
    return [pl.BlockSpec(memory_space=pltpu.VMEM)] * count


def small_call(kernel, out_shape, *operands):
    count = len(out_shape)
    return pl.pallas_call(
        kernel,
        out_shape=tuple(out_shape),
        in_specs=vmem_specs(len(operands)),
        out_specs=tuple(vmem_specs(count)),
        compiler_params=pltpu.CompilerParams(vmem_limit_bytes=SMALL_LIMIT),
    )(*operands)


def early(normed, cotangent, blocks):
    return pl.pallas_call(
        early_kernel,
        out_shape=(
            jax.ShapeDtypeStruct((D, 3 * HP), jnp.bfloat16),
            jax.ShapeDtypeStruct((TOK, 2 * HP), jnp.float32),
            jax.ShapeDtypeStruct((TOK, HP), jnp.float32),
        ),
        in_specs=vmem_specs(2 + len(blocks)),
        out_specs=tuple(vmem_specs(3)),
        compiler_params=pltpu.CompilerParams(vmem_limit_bytes=VMEM_LIMIT),
    )(normed, cotangent, *blocks)


def compute(*operands):
    half = jax.ShapeDtypeStruct((HALF, D), jnp.bfloat16)
    return pl.pallas_call(
        compute_kernel,
        out_shape=(
            half,
            half,
            jax.ShapeDtypeStruct((TOK, HP), jnp.bfloat16),
            jax.ShapeDtypeStruct((D, 3 * HP), jnp.bfloat16),
        ),
        in_specs=vmem_specs(len(operands)),
        out_specs=tuple(vmem_specs(4)),
        scratch_shapes=[
            pltpu.VMEM((TOK, D), jnp.bfloat16),
            pltpu.VMEM((256, 3 * HP), jnp.bfloat16),
        ],
        input_output_aliases={0: 3},
        compiler_params=pltpu.CompilerParams(vmem_limit_bytes=VMEM_LIMIT),
    )(*operands)


def turn(cotangent, normed):
    return pl.pallas_call(
        turn_kernel,
        out_shape=(
            jax.ShapeDtypeStruct((D, TOK), jnp.bfloat16),
            jax.ShapeDtypeStruct((256, TOK), jnp.bfloat16),
        ),
        in_specs=vmem_specs(2),
        out_specs=tuple(vmem_specs(2)),
        scratch_shapes=[pltpu.VMEM((D, TOK), jnp.bfloat16)],
        compiler_params=pltpu.CompilerParams(vmem_limit_bytes=SMALL_LIMIT),
    )(cotangent, normed)


def down_product(turned, hidden):
    return pl.pallas_call(
        down_kernel,
        out_shape=jax.ShapeDtypeStruct((D, HP), jnp.bfloat16),
        in_specs=vmem_specs(2),
        out_specs=pl.BlockSpec(memory_space=pltpu.HBM),
        scratch_shapes=[pltpu.VMEM((D, HP), jnp.bfloat16), pltpu.SemaphoreType.DMA((8,))],
        compiler_params=pltpu.CompilerParams(vmem_limit_bytes=DOWN_LIMIT),
    )(turned, hidden)


def pair_kernel(left_ref, right_ref, *out_refs):
    total = left_ref[...].astype(jnp.float32) + right_ref[...].astype(jnp.float32)
    rows = total.shape[0] // len(out_refs)
    for k, out in enumerate(out_refs):
        out[...] = total[k * rows : (k + 1) * rows].astype(jnp.bfloat16)


def final_kernel(x_ref, gain_ref, left1, right1, left2, right2, out_ref):
    gain = gain_ref[...]
    for k in range(4):
        rows = pl.ds(k * QUARTER, QUARTER)
        part = pl.ds(k % 2 * QUARTER, QUARTER)
        left, right = ((left1, right1), (left2, right2))[k // 2]
        value = x_ref[rows, :].astype(jnp.float32)
        inverse = lax.rsqrt(jnp.mean(value * value, axis=-1, keepdims=True) + EPSILON)
        normalized = value * inverse
        total = left[part, :].astype(jnp.float32) + right[part, :].astype(jnp.float32)
        scaled = total * gain
        mean = jnp.mean(scaled * normalized, axis=-1, keepdims=True)
        out_ref[rows, :] = (inverse * (scaled - normalized * mean)).astype(jnp.bfloat16)


def place_kernel(mine_ref, away_ref, out_ref, sems):
    c = lax.axis_index("c")
    copies = [
        pltpu.make_async_copy(ref, out_ref.at[half_rows(core), :], sems.at[k])
        for k, (core, ref) in enumerate(((c, mine_ref), (1 - c, away_ref)))
    ]
    for copy in copies:
        copy.start()
    for copy in copies:
        copy.wait()


def place(mine, away):
    return pl.pallas_call(
        place_kernel,
        out_shape=jax.ShapeDtypeStruct((TOK, D), jnp.bfloat16),
        in_specs=vmem_specs(2),
        out_specs=pl.BlockSpec(memory_space=pltpu.HBM),
        scratch_shapes=[pltpu.SemaphoreType.DMA((2,))],
        compiler_params=pltpu.CompilerParams(vmem_limit_bytes=SMALL_LIMIT),
    )(mine, away)


def sum_kernel(parts_ref, out_ref):
    total = parts_ref[0].astype(jnp.float32)
    for k in range(1, 8):
        total = total + parts_ref[k].astype(jnp.float32)
    out_ref[...] = total[:, : out_ref.shape[1]].astype(out_ref.dtype)


def with_partner(array, first):
    pairs = [
        (device_number(z, y, x, c), device_number(z, y, x ^ (1 if (c == 0) == first else 3), c))
        for z in range(NZ)
        for y in range(NY)
        for x in range(NX)
        for c in range(NC)
    ]
    return lax.ppermute(array, AXES, pairs)


def with_core(array):
    return lax.ppermute(array, "c", [(0, 1), (1, 0)])


def shards(inputs, gain, w_gate, w_up, w_down, cotangent):
    pad = ((0, 0), (0, HP - HU))
    packed = jnp.concatenate([jnp.pad(w, pad) for w in (w_gate, w_up, w_down.T)], axis=1)
    block = exchange(jnp.broadcast_to(packed[None], (8, DROWS, 3 * HP)), False)
    b0 = block.reshape(256, 3 * HP)
    p2 = ring(b0, 2)
    m2 = ring(b0, -2)
    p1 = ring(b0, 1)
    m1 = ring(b0, -1)
    p3 = ring(p2, 1)
    m3 = ring(m2, -1)
    p4 = ring(p2[:128], 2)
    m4 = ring(m2[128:], -2)

    row = gain.reshape(1, D)
    half = jax.ShapeDtypeStruct((HALF, D), jnp.bfloat16)
    normed, x_half = small_call(
        normalize_kernel, [jax.ShapeDtypeStruct((TOK, D), jnp.bfloat16), half], inputs, row
    )
    turned, last_x = turn(cotangent, normed)
    weights, gate_up, d_hidden = early(normed, cotangent, (b0, p1, p2, p3, m1, m2, m3))
    keep, send, hidden, _ = compute(weights, gate_up, d_hidden, last_x, turned, p4, m4)
    other = with_core(send)
    down = down_product(turned, hidden)
    arrived = exchange(down.reshape(8, 256, HP), True)
    (line,) = small_call(sum_kernel, [jax.ShapeDtypeStruct((256, HP), jnp.bfloat16)], arrived)
    arrived = exchange(line.reshape(8, DROWS, HP), False)
    (total,) = small_call(sum_kernel, [jax.ShapeDtypeStruct((DROWS, HU), jnp.float32)], arrived)
    grad_down = total.T

    piece = jax.ShapeDtypeStruct((HALF // 2, D), jnp.bfloat16)
    chip1, chip2 = small_call(pair_kernel, [piece, piece], keep, other)
    got1 = with_partner(chip1, True)
    got2 = with_partner(chip2, True)
    (two1,) = small_call(pair_kernel, [piece], chip1, got1)
    far1 = with_partner(two1, False)
    (two2,) = small_call(pair_kernel, [piece], chip2, got2)
    far2 = with_partner(two2, False)
    (mine,) = small_call(final_kernel, [half], x_half, row, two1, far1, two2, far2)
    away = with_core(mine)
    whole = place(mine, away)
    return whole, grad_down


def solution(mesh):
    split = Mesh(mesh.devices.reshape(NZ, NY, NX, NC), AXES)
    in_specs = (P(FS, None), P(), P(FS, TP), P(FS, TP), P(TP, FS), P(FS, None))
    out_specs = (P(FS, None), P(TP, FS))
    return jax.shard_map(
        shards, mesh=split, in_specs=in_specs, out_specs=out_specs, check_vma=False
    )
```

profile of v0, /device:TPU:1, one launch (start us, length us, event | category | flops | bytes accessed | tf_op | source)
XLA Modules:
  0.0 132.9 jit_solution(688295481054087150)
XLA Ops:
  0.7 0.9 fusion.5
  1.6 23.5 %all_to_all.15 = bf16[8,32,1152]{2,1,0:T(8,128)(2,1)S(1)} all-to-all(bf16[8,32,1152]{2,1,0:T(8,128)(2,1)S(1)} %broadcast_in_dim.2), channel_id=1, replica_groups={{0,8,16,24,32,40,48,56},{64,72,80,88,96,104,112,120},{128,136,144,152,1..., dimensions={0} | all-to-all | bytes 1179648 | tf_op jit(solution)/shard_map/all_to_all | solution.py:62
  25.1 6.0 %collective-permute-start.4 = (bf16[256,1152]{1,0:T(8,128)(2,1)S(1)}, bf16[256,1152]{1,0:T(8,128)(2,1)S(1)}, u32[]{:S(2)}, u32[]{:S(2)}) collective-permute-start(bf16[256,1152]{1,0:T(8,128)(2,1)S(1)} %bitcast.6), channel_id=1, source_target_pairs={{0,384},{1,49},{2,386},{3,51},{4,388},{5,53},{6,390},{7,55},{8,392... | collective-permute-start | bytes 1769480 | tf_op jit(solution)/shard_map/ppermute | solution.py:58
  31.1 1.9 %collective-permute-start.1 = (bf16[256,1152]{1,0:T(8,128)(2,1)S(1)}, bf16[256,1152]{1,0:T(8,128)(2,1)S(1)}, u32[]{:S(2)}, u32[]{:S(2)}) collective-permute-start(bf16[256,1152]{1,0:T(8,128)(2,1)S(1)} %bitcast.7), channel_id=1, source_target_pairs={{0,128},{1,17},{2,130},{3,19},{4,132},{5,21},{6,134},{7,23},{8,136... | collective-permute-start | bytes 1769480 | tf_op jit(solution)/shard_map/ppermute | solution.py:58
  33.0 4.7 %collective-permute-start.3 = (bf16[256,1152]{1,0:T(8,128)(2,1)S(1)}, bf16[256,1152]{1,0:T(8,128)(2,1)S(1)}, u32[]{:S(2)}, u32[]{:S(2)}) collective-permute-start(bf16[256,1152]{1,0:T(8,128)(2,1)S(1)} %bitcast.8), channel_id=1, source_target_pairs={{0,448},{1,57},{2,450},{3,59},{4,452},{5,61},{6,454},{7,63},{8,456... | collective-permute-start | bytes 1769480 | tf_op jit(solution)/shard_map/ppermute | solution.py:58
  37.7 1.9 %collective-permute-start = (bf16[256,1152]{1,0:T(8,128)(2,1)S(1)}, bf16[256,1152]{1,0:T(8,128)(2,1)S(1)}, u32[]{:S(2)}, u32[]{:S(2)}) collective-permute-start(bf16[256,1152]{1,0:T(8,128)(2,1)S(1)} %bitcast.9), channel_id=1, source_target_pairs={{0,64},{1,9},{2,66},{3,11},{4,68},{5,13},{6,70},{7,15},{8,72},{9,1... | collective-permute-start | bytes 1769480 | tf_op jit(solution)/shard_map/ppermute | solution.py:58
  39.7 4.6 %collective-permute-done.4.m2 = bf16[256,1152]{1,0:T(8,128)(2,1)S(1)} collective-permute-done((bf16[256,1152]{1,0:T(8,128)(2,1)S(1)}, bf16[256,1152]{1,0:T(8,128)(2,1)S(1)}, u32[]{:S(2)}, u32[]{:S(2)}) %collective-permute-start.4) | collective-permute-done | bytes 589856 | tf_op jit(solution)/shard_map/ppermute | solution.py:58
  44.2 4.4 %collective-permute-start.5 = (bf16[256,1152]{1,0:T(8,128)(2,1)S(1)}, bf16[256,1152]{1,0:T(8,128)(2,1)S(1)}, u32[]{:S(2)}, u32[]{:S(2)}) collective-permute-start(bf16[256,1152]{1,0:T(8,128)(2,1)S(1)} %collective-permute-done.4.m2), channel_id=1, source_target_pairs={{0,448},{1,57},{2,450},{3,59},{4,452},{5,61},{6,454},{7,63},{8,456... | collective-permute-start | bytes 1769480 | tf_op jit(solution)/shard_map/ppermute | solution.py:58
  48.7 4.1 %collective-permute-start.2 = (bf16[256,1152]{1,0:T(8,128)(2,1)S(1)}, bf16[256,1152]{1,0:T(8,128)(2,1)S(1)}, u32[]{:S(2)}, u32[]{:S(2)}) collective-permute-start(bf16[256,1152]{1,0:T(8,128)(2,1)S(1)} %collective-permute-done.1.p2), channel_id=1, source_target_pairs={{0,64},{1,9},{2,66},{3,11},{4,68},{5,13},{6,70},{7,15},{8,72},{9,1... | collective-permute-start | bytes 1769480 | tf_op jit(solution)/shard_map/ppermute | solution.py:58
  52.8 3.0 %collective-permute-start.7 = (bf16[128,1152]{1,0:T(8,128)(2,1)S(1)}, bf16[128,1152]{1,0:T(8,128)(2,1)S(1)}, u32[]{:S(2)}, u32[]{:S(2)}) collective-permute-start(bf16[128,1152]{1,0:T(8,128)(2,1)S(1)} %slice.9), channel_id=1, source_target_pairs={{0,384},{1,49},{2,386},{3,51},{4,388},{5,53},{6,390},{7,55},{8,392... | collective-permute-start | bytes 884744 | tf_op jit(solution)/shard_map/ppermute | solution.py:58
  55.8 3.2 %collective-permute-start.6 = (bf16[128,1152]{1,0:T(8,128)(2,1)S(1)}, bf16[128,1152]{1,0:T(8,128)(2,1)S(1)}, u32[]{:S(2)}, u32[]{:S(2)}) collective-permute-start(bf16[128,1152]{1,0:T(8,128)(2,1)S(1)} %slice.8), channel_id=1, source_target_pairs={{0,128},{1,17},{2,130},{3,19},{4,132},{5,21},{6,134},{7,23},{8,136... | collective-permute-start | bytes 884744 | tf_op jit(solution)/shard_map/ppermute | solution.py:58
  60.6 1.7 %collective-permute-done.2.p3 = bf16[256,1152]{1,0:T(8,128)(2,1)S(1)} collective-permute-done((bf16[256,1152]{1,0:T(8,128)(2,1)S(1)}, bf16[256,1152]{1,0:T(8,128)(2,1)S(1)}, u32[]{:S(2)}, u32[]{:S(2)}) %collective-permute-start.2) | collective-permute-done | bytes 589856 | tf_op jit(solution)/shard_map/ppermute | solution.py:58
  62.3 2.6 %shard_map.78 = (bf16[2048,1152]{1,0:T(8,128)(2,1)S(1)}, f32[384,768]{1,0:T(8,128)S(1)}, f32[384,384]{1,0:T(8,128)S(1)}) custom-call(bf16[384,2048]{1,0:T(8,128)(2,1)S(1)} %get-tuple-element.15.norm_ref, bf16[384,2048]{1,0:T(8,128)(2,1)S(1)} %copy-done, bf16[256,1152]{1,0:T(8,128)(2,1)S(1)} %bitcast.10, bf16[256,1152]{1,0:T(8,128)(2,1)S(1)} %collective-permute-done.p1, ...), custom_call_target="tpu_custom_call" | custom-call | tf_op jit(solution)/shard_map/pallas_call | solution.py:185
  64.9 2.4 %collective-permute-done.6.p4 = bf16[128,1152]{1,0:T(8,128)(2,1)S(1)} collective-permute-done((bf16[128,1152]{1,0:T(8,128)(2,1)S(1)}, bf16[128,1152]{1,0:T(8,128)(2,1)S(1)}, u32[]{:S(2)}, u32[]{:S(2)}) %collective-permute-start.6) | collective-permute-done | bytes 294944 | tf_op jit(solution)/shard_map/ppermute | solution.py:58
  67.3 2.3 %shard_map.80 = (bf16[192,2048]{1,0:T(8,128)(2,1)S(1)}, bf16[192,2048]{1,0:T(8,128)(2,1)S(1)}, bf16[384,384]{1,0:T(8,128)(2,1)S(1)}, bf16[2048,1152]{1,0:T(8,128)(2,1)S(1)}) custom-call(bf16[2048,1152]{1,0:T(8,128)(2,1)S(1)} %get-tuple-element.16.w_in, f32[384,768]{1,0:T(8,128)S(1)} %get-tuple-element.17.gate_up_ref, ...), custom_call_target="tpu_custom_call", output_to_operand_aliasing={{3}: (0, {})} | custom-call | tf_op jit(solution)/shard_map/pallas_call | solution.py:200
  69.5 1.9 %shard_map.86 = bf16[2048,384]{1,0:T(8,128)(2,1)} custom-call(bf16[2048,384]{1,0:T(8,128)(2,1)S(1)} %get-tuple-element.20.turned_cot.turned_ref, bf16[384,384]{1,0:T(8,128)(2,1)S(1)} %get-tuple-element.25.hidden_ref), custom_call_target="tpu_custom_call" | custom-call | tf_op jit(solution)/shard_map/pallas_call | solution.py:234
  71.4 5.2 %all-to-all-start.1 = ((bf16[8,256,384]{2,1,0:T(8,128)(2,1)}), bf16[8,256,384]{2,1,0:T(8,128)(2,1)S(1)}, u32[]{:S(2)}, u32[]{:S(2)}) async-start(bf16[8,256,384]{2,1,0:T(8,128)(2,1)} %bitcast.3), calls=%async_computation.1 | async-start | bytes 3145728 | tf_op jit(solution)/shard_map/all_to_all | solution.py:62
  76.6 8.4 %collective-permute-start.8 = (bf16[192,2048]{1,0:T(8,128)(2,1)}, bf16[192,2048]{1,0:T(8,128)(2,1)S(1)}, u32[]{:S(2)}, u32[]{:S(2)}) collective-permute-start(bf16[192,2048]{1,0:T(8,128)(2,1)} %copy-done.3), channel_id=1, source_target_pairs={{0,1},{1,0},{2,3},{3,2},{4,5},{5,4},{6,7},{7,6},{8,9},{9,8},{10,11... | collective-permute-start | bytes 2359304 | tf_op jit(solution)/shard_map/ppermute | solution.py:308
  85.0 2.1 %collective-permute-done.8.right_ref = bf16[192,2048]{1,0:T(8,128)(2,1)S(1)} collective-permute-done((bf16[192,2048]{1,0:T(8,128)(2,1)}, bf16[192,2048]{1,0:T(8,128)(2,1)S(1)}, u32[]{:S(2)}, u32[]{:S(2)}) %collective-permute-start.8) | collective-permute-done | bytes 786464 | tf_op jit(solution)/shard_map/ppermute | solution.py:308
  87.3 4.4 %collective-permute-start.9 = (bf16[96,2048]{1,0:T(8,128)(2,1)S(1)}, bf16[96,2048]{1,0:T(8,128)(2,1)S(1)}, u32[]{:S(2)}, u32[]{:S(2)}) collective-permute-start(bf16[96,2048]{1,0:T(8,128)(2,1)S(1)} %get-tuple-element.23.left_ref), channel_id=1, source_target_pairs={{0,2},{1,7},{2,0},{3,5},{4,6},{5,3},{6,4},{7,1},{8,10},{9,15},{10,... | collective-permute-start | bytes 1179656 | tf_op jit(solution)/shard_map/ppermute | solution.py:304
  91.7 2.1 %collective-permute-start.11 = (bf16[96,2048]{1,0:T(8,128)(2,1)S(1)}, bf16[96,2048]{1,0:T(8,128)(2,1)S(1)}, u32[]{:S(2)}, u32[]{:S(2)}) collective-permute-start(bf16[96,2048]{1,0:T(8,128)(2,1)S(1)} %get-tuple-element.24.left_ref), channel_id=1, source_target_pairs={{0,2},{1,7},{2,0},{3,5},{4,6},{5,3},{6,4},{7,1},{8,10},{9,15},{10,... | collective-permute-start | bytes 1179656 | tf_op jit(solution)/shard_map/ppermute | solution.py:304
  93.8 3.5 %collective-permute-done.9.right_ref = bf16[96,2048]{1,0:T(8,128)(2,1)S(1)} collective-permute-done((bf16[96,2048]{1,0:T(8,128)(2,1)S(1)}, bf16[96,2048]{1,0:T(8,128)(2,1)S(1)}, u32[]{:S(2)}, u32[]{:S(2)}) %collective-permute-start.9) | collective-permute-done | bytes 393248 | tf_op jit(solution)/shard_map/ppermute | solution.py:304
  97.4 1.9 %collective-permute-start.10 = (bf16[96,2048]{1,0:T(8,128)(2,1)S(1)}, bf16[96,2048]{1,0:T(8,128)(2,1)S(1)}, u32[]{:S(2)}, u32[]{:S(2)}) collective-permute-start(bf16[96,2048]{1,0:T(8,128)(2,1)S(1)} %shard_map.82.left1), channel_id=1, source_target_pairs={{0,6},{1,3},{2,4},{3,1},{4,2},{5,7},{6,0},{7,5},{8,14},{9,11},{10,... | collective-permute-start | bytes 1179656 | tf_op jit(solution)/shard_map/ppermute | solution.py:304
  99.4 2.1 %collective-permute-done.11.right_ref = bf16[96,2048]{1,0:T(8,128)(2,1)S(1)} collective-permute-done((bf16[96,2048]{1,0:T(8,128)(2,1)S(1)}, bf16[96,2048]{1,0:T(8,128)(2,1)S(1)}, u32[]{:S(2)}, u32[]{:S(2)}) %collective-permute-start.11) | collective-permute-done | bytes 393248 | tf_op jit(solution)/shard_map/ppermute | solution.py:304
  101.5 2.0 %collective-permute-start.12 = (bf16[96,2048]{1,0:T(8,128)(2,1)S(1)}, bf16[96,2048]{1,0:T(8,128)(2,1)S(1)}, u32[]{:S(2)}, u32[]{:S(2)}) collective-permute-start(bf16[96,2048]{1,0:T(8,128)(2,1)S(1)} %shard_map.83.left2), channel_id=1, source_target_pairs={{0,6},{1,3},{2,4},{3,1},{4,2},{5,7},{6,0},{7,5},{8,14},{9,11},{10,... | collective-permute-start | bytes 1179656 | tf_op jit(solution)/shard_map/ppermute | solution.py:304
  103.6 2.7 %collective-permute-done.10.right1 = bf16[96,2048]{1,0:T(8,128)(2,1)S(1)} collective-permute-done((bf16[96,2048]{1,0:T(8,128)(2,1)S(1)}, bf16[96,2048]{1,0:T(8,128)(2,1)S(1)}, u32[]{:S(2)}, u32[]{:S(2)}) %collective-permute-start.10) | collective-permute-done | bytes 393248 | tf_op jit(solution)/shard_map/ppermute | solution.py:304
  106.3 4.2 %collective-permute-done.12.right2 = bf16[96,2048]{1,0:T(8,128)(2,1)S(1)} collective-permute-done((bf16[96,2048]{1,0:T(8,128)(2,1)S(1)}, bf16[96,2048]{1,0:T(8,128)(2,1)S(1)}, u32[]{:S(2)}, u32[]{:S(2)}) %collective-permute-start.12) | collective-permute-done | bytes 393248 | tf_op jit(solution)/shard_map/ppermute | solution.py:304
  111.3 4.5 %collective-permute-start.13 = (bf16[192,2048]{1,0:T(8,128)(2,1)S(1)}, bf16[192,2048]{1,0:T(8,128)(2,1)S(1)}, u32[]{:S(2)}, u32[]{:S(2)}) collective-permute-start(bf16[192,2048]{1,0:T(8,128)(2,1)S(1)} %shard_map.84.mine_ref), channel_id=1, source_target_pairs={{0,1},{1,0},{2,3},{3,2},{4,5},{5,4},{6,7},{7,6},{8,9},{9,8},{10,11... | collective-permute-start | bytes 2359304 | tf_op jit(solution)/shard_map/ppermute | solution.py:308
  115.8 0.9 shard_map.87
  116.7 6.9 %all-to-all-start.2 = ((bf16[8,32,384]{2,1,0:T(8,128)(2,1)}), bf16[8,32,384]{2,1,0:T(8,128)(2,1)S(1)}, u32[]{:S(2)}, u32[]{:S(2)}) async-start(bf16[8,32,384]{2,1,0:T(8,128)(2,1)} %bitcast.4), calls=%async_computation.2 | async-start | bytes 393216 | tf_op jit(solution)/shard_map/all_to_all | solution.py:62
  123.6 1.2 shard_map.85
  124.8 7.5 %all-to-all-done.2.parts_ref = bf16[8,32,384]{2,1,0:T(8,128)(2,1)S(1)} async-done(((bf16[8,32,384]{2,1,0:T(8,128)(2,1)}), bf16[8,32,384]{2,1,0:T(8,128)(2,1)S(1)}, u32[]{:S(2)}, u32[]{:S(2)}) %all-to-all-start.2) | async-done | bytes 196640 | tf_op jit(solution)/shard_map/all_to_all | solution.py:62
  (25 shorter events, 3.5 us)
Async XLA Ops:
  0.6 58.4 %copy-start.1 = (bf16[384,2048]{1,0:T(8,128)(2,1)S(1)}, bf16[384,2048]{1,0:T(8,128)(2,1)}, u32[]{:S(2)}) copy-start(bf16[384,2048]{1,0:T(8,128)(2,1)} %x_ref.1) | copy-start | bytes 4718596
  0.6 58.4 %copy-start.2 = (f32[2048]{0:T(1024)S(1)}, f32[2048]{0:T(1024)}, u32[]{:S(2)}) copy-start(f32[2048]{0:T(1024)} %param.7) | copy-start | bytes 24580
  25.1 34.6 %copy-start = (bf16[384,2048]{1,0:T(8,128)(2,1)S(1)}, bf16[384,2048]{1,0:T(8,128)(2,1)}, u32[]{:S(2)}) copy-start(bf16[384,2048]{1,0:T(8,128)(2,1)} %cot_ref.3) | copy-start | bytes 4718596
  25.1 19.1 %collective-permute-start.4 = (bf16[256,1152]{1,0:T(8,128)(2,1)S(1)}, bf16[256,1152]{1,0:T(8,128)(2,1)S(1)}, u32[]{:S(2)}, u32[]{:S(2)}) collective-permute-start(bf16[256,1152]{1,0:T(8,128)(2,1)S(1)} %bitcast.6), channel_id=1, source_target_pairs={{0,384},{1,49},{2,386},{3,51},{4,388},{5,53},{6,390},{7,55},{8,392... | collective-permute-start | bytes 1769480 | tf_op jit(solution)/shard_map/ppermute | solution.py:58
  31.1 17.5 %collective-permute-start.1 = (bf16[256,1152]{1,0:T(8,128)(2,1)S(1)}, bf16[256,1152]{1,0:T(8,128)(2,1)S(1)}, u32[]{:S(2)}, u32[]{:S(2)}) collective-permute-start(bf16[256,1152]{1,0:T(8,128)(2,1)S(1)} %bitcast.7), channel_id=1, source_target_pairs={{0,128},{1,17},{2,130},{3,19},{4,132},{5,21},{6,134},{7,23},{8,136... | collective-permute-start | bytes 1769480 | tf_op jit(solution)/shard_map/ppermute | solution.py:58
  33.0 22.8 %collective-permute-start.3 = (bf16[256,1152]{1,0:T(8,128)(2,1)S(1)}, bf16[256,1152]{1,0:T(8,128)(2,1)S(1)}, u32[]{:S(2)}, u32[]{:S(2)}) collective-permute-start(bf16[256,1152]{1,0:T(8,128)(2,1)S(1)} %bitcast.8), channel_id=1, source_target_pairs={{0,448},{1,57},{2,450},{3,59},{4,452},{5,61},{6,454},{7,63},{8,456... | collective-permute-start | bytes 1769480 | tf_op jit(solution)/shard_map/ppermute | solution.py:58
  37.7 22.9 %collective-permute-start = (bf16[256,1152]{1,0:T(8,128)(2,1)S(1)}, bf16[256,1152]{1,0:T(8,128)(2,1)S(1)}, u32[]{:S(2)}, u32[]{:S(2)}) collective-permute-start(bf16[256,1152]{1,0:T(8,128)(2,1)S(1)} %bitcast.9), channel_id=1, source_target_pairs={{0,64},{1,9},{2,66},{3,11},{4,68},{5,13},{6,70},{7,15},{8,72},{9,1... | collective-permute-start | bytes 1769480 | tf_op jit(solution)/shard_map/ppermute | solution.py:58
  44.2 16.4 %collective-permute-start.5 = (bf16[256,1152]{1,0:T(8,128)(2,1)S(1)}, bf16[256,1152]{1,0:T(8,128)(2,1)S(1)}, u32[]{:S(2)}, u32[]{:S(2)}) collective-permute-start(bf16[256,1152]{1,0:T(8,128)(2,1)S(1)} %collective-permute-done.4.m2), channel_id=1, source_target_pairs={{0,448},{1,57},{2,450},{3,59},{4,452},{5,61},{6,454},{7,63},{8,456... | collective-permute-start | bytes 1769480 | tf_op jit(solution)/shard_map/ppermute | solution.py:58
  48.7 13.7 %collective-permute-start.2 = (bf16[256,1152]{1,0:T(8,128)(2,1)S(1)}, bf16[256,1152]{1,0:T(8,128)(2,1)S(1)}, u32[]{:S(2)}, u32[]{:S(2)}) collective-permute-start(bf16[256,1152]{1,0:T(8,128)(2,1)S(1)} %collective-permute-done.1.p2), channel_id=1, source_target_pairs={{0,64},{1,9},{2,66},{3,11},{4,68},{5,13},{6,70},{7,15},{8,72},{9,1... | collective-permute-start | bytes 1769480 | tf_op jit(solution)/shard_map/ppermute | solution.py:58
  52.8 12.1 %collective-permute-start.7 = (bf16[128,1152]{1,0:T(8,128)(2,1)S(1)}, bf16[128,1152]{1,0:T(8,128)(2,1)S(1)}, u32[]{:S(2)}, u32[]{:S(2)}) collective-permute-start(bf16[128,1152]{1,0:T(8,128)(2,1)S(1)} %slice.9), channel_id=1, source_target_pairs={{0,384},{1,49},{2,386},{3,51},{4,388},{5,53},{6,390},{7,55},{8,392... | collective-permute-start | bytes 884744 | tf_op jit(solution)/shard_map/ppermute | solution.py:58
  55.8 11.4 %collective-permute-start.6 = (bf16[128,1152]{1,0:T(8,128)(2,1)S(1)}, bf16[128,1152]{1,0:T(8,128)(2,1)S(1)}, u32[]{:S(2)}, u32[]{:S(2)}) collective-permute-start(bf16[128,1152]{1,0:T(8,128)(2,1)S(1)} %slice.8), channel_id=1, source_target_pairs={{0,128},{1,17},{2,130},{3,19},{4,132},{5,21},{6,134},{7,23},{8,136... | collective-permute-start | bytes 884744 | tf_op jit(solution)/shard_map/ppermute | solution.py:58
  69.5 1.9 %copy-start.3 = (bf16[192,2048]{1,0:T(8,128)(2,1)}, bf16[192,2048]{1,0:T(8,128)(2,1)S(1)}, u32[]{:S(2)}) copy-start(bf16[192,2048]{1,0:T(8,128)(2,1)S(1)} %get-tuple-element.22) | copy-start | bytes 2359300
  71.4 44.4 %all-to-all-start.1 = ((bf16[8,256,384]{2,1,0:T(8,128)(2,1)}), bf16[8,256,384]{2,1,0:T(8,128)(2,1)S(1)}, u32[]{:S(2)}, u32[]{:S(2)}) async-start(bf16[8,256,384]{2,1,0:T(8,128)(2,1)} %bitcast.3), calls=%async_computation.1 | async-start | bytes 3145728 | tf_op jit(solution)/shard_map/all_to_all | solution.py:62
  76.6 10.5 %collective-permute-start.8 = (bf16[192,2048]{1,0:T(8,128)(2,1)}, bf16[192,2048]{1,0:T(8,128)(2,1)S(1)}, u32[]{:S(2)}, u32[]{:S(2)}) collective-permute-start(bf16[192,2048]{1,0:T(8,128)(2,1)} %copy-done.3), channel_id=1, source_target_pairs={{0,1},{1,0},{2,3},{3,2},{4,5},{5,4},{6,7},{7,6},{8,9},{9,8},{10,11... | collective-permute-start | bytes 2359304 | tf_op jit(solution)/shard_map/ppermute | solution.py:308
  87.3 10.0 %collective-permute-start.9 = (bf16[96,2048]{1,0:T(8,128)(2,1)S(1)}, bf16[96,2048]{1,0:T(8,128)(2,1)S(1)}, u32[]{:S(2)}, u32[]{:S(2)}) collective-permute-start(bf16[96,2048]{1,0:T(8,128)(2,1)S(1)} %get-tuple-element.23.left_ref), channel_id=1, source_target_pairs={{0,2},{1,7},{2,0},{3,5},{4,6},{5,3},{6,4},{7,1},{8,10},{9,15},{10,... | collective-permute-start | bytes 1179656 | tf_op jit(solution)/shard_map/ppermute | solution.py:304
  91.7 9.7 %collective-permute-start.11 = (bf16[96,2048]{1,0:T(8,128)(2,1)S(1)}, bf16[96,2048]{1,0:T(8,128)(2,1)S(1)}, u32[]{:S(2)}, u32[]{:S(2)}) collective-permute-start(bf16[96,2048]{1,0:T(8,128)(2,1)S(1)} %get-tuple-element.24.left_ref), channel_id=1, source_target_pairs={{0,2},{1,7},{2,0},{3,5},{4,6},{5,3},{6,4},{7,1},{8,10},{9,15},{10,... | collective-permute-start | bytes 1179656 | tf_op jit(solution)/shard_map/ppermute | solution.py:304
  97.4 8.8 %collective-permute-start.10 = (bf16[96,2048]{1,0:T(8,128)(2,1)S(1)}, bf16[96,2048]{1,0:T(8,128)(2,1)S(1)}, u32[]{:S(2)}, u32[]{:S(2)}) collective-permute-start(bf16[96,2048]{1,0:T(8,128)(2,1)S(1)} %shard_map.82.left1), channel_id=1, source_target_pairs={{0,6},{1,3},{2,4},{3,1},{4,2},{5,7},{6,0},{7,5},{8,14},{9,11},{10,... | collective-permute-start | bytes 1179656 | tf_op jit(solution)/shard_map/ppermute | solution.py:304
  101.5 8.9 %collective-permute-start.12 = (bf16[96,2048]{1,0:T(8,128)(2,1)S(1)}, bf16[96,2048]{1,0:T(8,128)(2,1)S(1)}, u32[]{:S(2)}, u32[]{:S(2)}) collective-permute-start(bf16[96,2048]{1,0:T(8,128)(2,1)S(1)} %shard_map.83.left2), channel_id=1, source_target_pairs={{0,6},{1,3},{2,4},{3,1},{4,2},{5,7},{6,0},{7,5},{8,14},{9,11},{10,... | collective-permute-start | bytes 1179656 | tf_op jit(solution)/shard_map/ppermute | solution.py:304
  111.3 12.4 %collective-permute-start.13 = (bf16[192,2048]{1,0:T(8,128)(2,1)S(1)}, bf16[192,2048]{1,0:T(8,128)(2,1)S(1)}, u32[]{:S(2)}, u32[]{:S(2)}) collective-permute-start(bf16[192,2048]{1,0:T(8,128)(2,1)S(1)} %shard_map.84.mine_ref), channel_id=1, source_target_pairs={{0,1},{1,0},{2,3},{3,2},{4,5},{5,4},{6,7},{7,6},{8,9},{9,8},{10,11... | collective-permute-start | bytes 2359304 | tf_op jit(solution)/shard_map/ppermute | solution.py:308
  116.7 15.6 %all-to-all-start.2 = ((bf16[8,32,384]{2,1,0:T(8,128)(2,1)}), bf16[8,32,384]{2,1,0:T(8,128)(2,1)S(1)}, u32[]{:S(2)}, u32[]{:S(2)}) async-start(bf16[8,32,384]{2,1,0:T(8,128)(2,1)} %bitcast.4), calls=%async_computation.2 | async-start | bytes 393216 | tf_op jit(solution)/shard_map/all_to_all | solution.py:62
where the time goes:
time: 134 us; the launch traced here: 133 us
  starting transfers between devices  64.7 us (48%)
  waiting for transfers between devices  30.7 us (23%)
  blocking collectives  23.5 us (18%)
  Pallas kernels  12 us (9%)
    ppermute x8, starting transfers between devices, ring(): return lax.ppermute(array, AXES, ring_pairs(step))  29.2 us
    all_to_all x1, blocking collectives, exchange(): lax.all_to_all(array, AXES, 0, 0, axis_index_groups=line_groups(along_rin...  23.5 us
    ppermute x2, starting transfers between devices, with_core(): return lax.ppermute(array, 'c', [(0, 1), (1, 0)])  13 us
    ppermute x4, waiting for transfers between devices, with_partner(): return lax.ppermute(array, AXES, pairs)  12.5 us
    all_to_all x2, starting transfers between devices, exchange(): lax.all_to_all(array, AXES, 0, 0, axis_index_groups=line_groups(along_rin...  12.1 us
    ppermute x4, starting transfers between devices, with_partner(): return lax.ppermute(array, AXES, pairs)  10.4 us
    ppermute x8, waiting for transfers between devices, ring(): return lax.ppermute(array, AXES, ring_pairs(step))  8.66 us
    all_to_all x2, waiting for transfers between devices, exchange(): lax.all_to_all(array, AXES, 0, 0, axis_index_groups=line_groups(along_rin...  7.46 us
  transfers between devices with their start and end apart: 16, of which 9 were waited for; matrix products, arithmetic and copies ran while one was open for 0% of the time, Pallas kernels for 5%

commit v1 on v0

--- a/solution.py
+++ b/solution.py
@@ -19,7 +19,6 @@
 HP = 384
 DROWS = 32
 HALF = TOK // NC
-QUARTER = HALF // NX
 VMEM_LIMIT = 28 * 2**20
 SMALL_LIMIT = 6 * 2**20
 DOWN_LIMIT = 16 * 2**20
@@ -108,7 +107,7 @@
 
 def compute_kernel(
     w_in, gate_up_ref, d_hidden_ref, turned_x, turned_cot, p4, m4,
-    keep_ref, send_ref, hidden_ref, w_ref, part_ref, last_ref,
+    keep_ref, send_ref, hidden_ref, w_ref, part_ref, last_ref, sum_ref, both_ref,
 ):
     c = lax.axis_index("c")
     r = ring_place()
@@ -118,18 +117,19 @@
         w_ref[block_rows(r + 4, o), :] = last_ref[pl.ds(o * DROWS, DROWS), :]
 
     last = pl.ds(pl.multiple_of(lax.rem(r + 4, 8) * 256, 256), 256)
-    gate_up = gate_up_ref[...] + dot(turned_x[...], last_ref[:, : 2 * HP], ((0,), (0,)))
-    gate = gate_up[:, :HP]
-    up = gate_up[:, HP:]
-    d_hidden = d_hidden_ref[...] + dot(turned_cot[last, :], last_ref[:, 2 * HP :], ((0,), (0,)))
-    d_hidden = HALF_STEP * d_hidden
-    sig = jax.nn.sigmoid(gate)
-    hidden = (gate * sig * up).astype(jnp.bfloat16)
-    d_gate = (d_hidden * up * sig * (1.0 + gate * (1.0 - sig))).astype(jnp.bfloat16)
-    d_up = (d_hidden * gate * sig).astype(jnp.bfloat16)
-    both = jnp.concatenate([d_gate, d_up], axis=1)
-    part_ref[...] = dot(both, w_ref[:, : 2 * HP], ((1,), (1,))).astype(jnp.bfloat16)
-    hidden_ref[...] = hidden
+    sum_ref[:, : 2 * HP] = dot(turned_x[...], last_ref[:, : 2 * HP], ((0,), (0,)))
+    sum_ref[:, 2 * HP :] = dot(turned_cot[last, :], last_ref[:, 2 * HP :], ((0,), (0,)))
+    for k in range(TOK // 32):
+        rows = pl.ds(k * 32, 32)
+        gate = gate_up_ref[rows, :HP] + sum_ref[rows, :HP]
+        up = gate_up_ref[rows, HP:] + sum_ref[rows, HP : 2 * HP]
+        d_hidden = HALF_STEP * (d_hidden_ref[rows, :] + sum_ref[rows, 2 * HP :])
+        sig = jax.nn.sigmoid(gate)
+        hidden_ref[rows, :] = (gate * sig * up).astype(jnp.bfloat16)
+        d_gate = d_hidden * up * sig * (1.0 + gate * (1.0 - sig))
+        both_ref[rows, :HP] = d_gate.astype(jnp.bfloat16)
+        both_ref[rows, HP:] = (d_hidden * gate * sig).astype(jnp.bfloat16)
+    part_ref[...] = dot(both_ref[...], w_ref[:, : 2 * HP], ((1,), (1,))).astype(jnp.bfloat16)
     keep_ref[...] = part_ref[half_rows(c), :]
     send_ref[...] = part_ref[half_rows(1 - c), :]
 
@@ -210,6 +210,8 @@
         scratch_shapes=[
             pltpu.VMEM((TOK, D), jnp.bfloat16),
             pltpu.VMEM((256, 3 * HP), jnp.bfloat16),
+            pltpu.VMEM((TOK, 3 * HP), jnp.float32),
+            pltpu.VMEM((TOK, 2 * HP), jnp.bfloat16),
         ],
         input_output_aliases={0: 3},
         compiler_params=pltpu.CompilerParams(vmem_limit_bytes=VMEM_LIMIT),
@@ -248,17 +250,23 @@
         out[...] = total[k * rows : (k + 1) * rows].astype(jnp.bfloat16)
 
 
-def final_kernel(x_ref, gain_ref, left1, right1, left2, right2, out_ref):
-    gain = gain_ref[...]
-    for k in range(4):
-        rows = pl.ds(k * QUARTER, QUARTER)
-        part = pl.ds(k % 2 * QUARTER, QUARTER)
-        left, right = ((left1, right1), (left2, right2))[k // 2]
+def inverse_kernel(x_ref, out_ref):
+    for k in range(HALF // 16):
+        rows = pl.ds(k * 16, 16)
         value = x_ref[rows, :].astype(jnp.float32)
         inverse = lax.rsqrt(jnp.mean(value * value, axis=-1, keepdims=True) + EPSILON)
-        normalized = value * inverse
+        out_ref[rows, :] = jnp.broadcast_to(inverse, (16, 128))
+
+
+def final_kernel(x_ref, inverse_ref, gain_ref, left1, right1, left2, right2, out_ref):
+    for k in range(HALF // 16):
+        rows = pl.ds(k * 16, 16)
+        part = pl.ds(k * 16 % (HALF // 2), 16)
+        left, right = ((left1, right1), (left2, right2))[k * 16 // (HALF // 2)]
+        inverse = inverse_ref[rows, :1]
+        normalized = x_ref[rows, :].astype(jnp.float32) * inverse
         total = left[part, :].astype(jnp.float32) + right[part, :].astype(jnp.float32)
-        scaled = total * gain
+        scaled = total * gain_ref[...]
         mean = jnp.mean(scaled * normalized, axis=-1, keepdims=True)
         out_ref[rows, :] = (inverse * (scaled - normalized * mean)).astype(jnp.bfloat16)
 
@@ -346,7 +354,10 @@
     far1 = with_partner(two1, False)
     (two2,) = small_call(pair_kernel, [piece], chip2, got2)
     far2 = with_partner(two2, False)
-    (mine,) = small_call(final_kernel, [half], x_half, row, two1, far1, two2, far2)
+    (inverse,) = small_call(
+        inverse_kernel, [jax.ShapeDtypeStruct((HALF, 128), jnp.float32)], x_half
+    )
+    (mine,) = small_call(final_kernel, [half], x_half, inverse, row, two1, far1, two2, far2)
     away = with_core(mine)
     whole = place(mine, away)
     return whole, grad_down

time: 134 us -> 132 us (0.985)
  starting transfers between devices: 64.7 us -> 62.8 us
    ppermute x2, starting transfers between devices: 13 us -> 11.4 us  [with_core(): return lax.ppermute(array, 'c', [(0, 1), (1, 0)])]
    pallas_call x7 -> x8, Pallas kernels: 3.33 us -> 3.66 us  [small_call(): pl.pallas_call(kernel, out_shape=tuple(out_shape), in_specs=vmem_specs(le...]
  transfers between devices with their start and end apart: 16 -> 16, of which waited for: 9 -> 10; matrix products, arithmetic and copies ran while one was open for 0% -> 0% of each run, Pallas kernels for 5% -> 6%
where the time goes in v1:
time: 132 us; the launch traced here: 131 us
  starting transfers between devices  62.8 us (48%)
  waiting for transfers between devices  30.8 us (23%)
  blocking collectives  23.5 us (18%)
  Pallas kernels  12.4 us (9%)
    ppermute x8, starting transfers between devices, ring(): return lax.ppermute(array, AXES, ring_pairs(step))  29.7 us
    all_to_all x1, blocking collectives, exchange(): lax.all_to_all(array, AXES, 0, 0, axis_index_groups=line_groups(along_rin...  23.5 us
    ppermute x4, waiting for transfers between devices, with_partner(): return lax.ppermute(array, AXES, pairs)  12.3 us
    ppermute x2, starting transfers between devices, with_core(): return lax.ppermute(array, 'c', [(0, 1), (1, 0)])  11.4 us
    all_to_all x2, starting transfers between devices, exchange(): lax.all_to_all(array, AXES, 0, 0, axis_index_groups=line_groups(along_rin...  11.3 us
    ppermute x4, starting transfers between devices, with_partner(): return lax.ppermute(array, AXES, pairs)  10.4 us
    ppermute x8, waiting for transfers between devices, ring(): return lax.ppermute(array, AXES, ring_pairs(step))  9.02 us
    all_to_all x2, waiting for transfers between devices, exchange(): lax.all_to_all(array, AXES, 0, 0, axis_index_groups=line_groups(along_rin...  7.46 us
  transfers between devices with their start and end apart: 16, of which 10 were waited for; matrix products, arithmetic and copies ran while one was open for 0% of the time, Pallas kernels for 6%

profile of v1, /device:TPU:1, one launch (start us, length us, event | category | flops | bytes accessed | tf_op | source)
XLA Modules:
  0.0 131.4 jit_solution(13746544121330438315)
XLA Ops:
  0.7 0.9 fusion.5
  1.6 23.5 %all_to_all.15 = bf16[8,32,1152]{2,1,0:T(8,128)(2,1)S(1)} all-to-all(bf16[8,32,1152]{2,1,0:T(8,128)(2,1)S(1)} %broadcast_in_dim.2), channel_id=1, replica_groups={{0,8,16,24,32,40,48,56},{64,72,80,88,96,104,112,120},{128,136,144,152,1..., dimensions={0} | all-to-all | bytes 1179648 | tf_op jit(solution)/shard_map/all_to_all | solution.py:61
  25.1 4.3 %collective-permute-start.1 = (bf16[256,1152]{1,0:T(8,128)(2,1)S(1)}, bf16[256,1152]{1,0:T(8,128)(2,1)S(1)}, u32[]{:S(2)}, u32[]{:S(2)}) collective-permute-start(bf16[256,1152]{1,0:T(8,128)(2,1)S(1)} %bitcast.6), channel_id=1, source_target_pairs={{0,128},{1,17},{2,130},{3,19},{4,132},{5,21},{6,134},{7,23},{8,136... | collective-permute-start | bytes 1769480 | tf_op jit(solution)/shard_map/ppermute | solution.py:57
  29.4 3.6 %collective-permute-start.4 = (bf16[256,1152]{1,0:T(8,128)(2,1)S(1)}, bf16[256,1152]{1,0:T(8,128)(2,1)S(1)}, u32[]{:S(2)}, u32[]{:S(2)}) collective-permute-start(bf16[256,1152]{1,0:T(8,128)(2,1)S(1)} %bitcast.7), channel_id=1, source_target_pairs={{0,384},{1,49},{2,386},{3,51},{4,388},{5,53},{6,390},{7,55},{8,392... | collective-permute-start | bytes 1769480 | tf_op jit(solution)/shard_map/ppermute | solution.py:57
  33.0 2.8 %collective-permute-start = (bf16[256,1152]{1,0:T(8,128)(2,1)S(1)}, bf16[256,1152]{1,0:T(8,128)(2,1)S(1)}, u32[]{:S(2)}, u32[]{:S(2)}) collective-permute-start(bf16[256,1152]{1,0:T(8,128)(2,1)S(1)} %bitcast.8), channel_id=1, source_target_pairs={{0,64},{1,9},{2,66},{3,11},{4,68},{5,13},{6,70},{7,15},{8,72},{9,1... | collective-permute-start | bytes 1769480 | tf_op jit(solution)/shard_map/ppermute | solution.py:57
  35.8 3.7 %collective-permute-start.3 = (bf16[256,1152]{1,0:T(8,128)(2,1)S(1)}, bf16[256,1152]{1,0:T(8,128)(2,1)S(1)}, u32[]{:S(2)}, u32[]{:S(2)}) collective-permute-start(bf16[256,1152]{1,0:T(8,128)(2,1)S(1)} %bitcast.9), channel_id=1, source_target_pairs={{0,448},{1,57},{2,450},{3,59},{4,452},{5,61},{6,454},{7,63},{8,456... | collective-permute-start | bytes 1769480 | tf_op jit(solution)/shard_map/ppermute | solution.py:57
  39.5 2.1 %collective-permute-done.1.p2 = bf16[256,1152]{1,0:T(8,128)(2,1)S(1)} collective-permute-done((bf16[256,1152]{1,0:T(8,128)(2,1)S(1)}, bf16[256,1152]{1,0:T(8,128)(2,1)S(1)}, u32[]{:S(2)}, u32[]{:S(2)}) %collective-permute-start.1) | collective-permute-done | bytes 589856 | tf_op jit(solution)/shard_map/ppermute | solution.py:57
  41.6 5.9 %collective-permute-start.2 = (bf16[256,1152]{1,0:T(8,128)(2,1)S(1)}, bf16[256,1152]{1,0:T(8,128)(2,1)S(1)}, u32[]{:S(2)}, u32[]{:S(2)}) collective-permute-start(bf16[256,1152]{1,0:T(8,128)(2,1)S(1)} %collective-permute-done.1.p2), channel_id=1, source_target_pairs={{0,64},{1,9},{2,66},{3,11},{4,68},{5,13},{6,70},{7,15},{8,72},{9,1... | collective-permute-start | bytes 1769480 | tf_op jit(solution)/shard_map/ppermute | solution.py:57
  47.6 1.2 collective-permute-done.4.m2
  48.8 1.9 %collective-permute-start.5 = (bf16[256,1152]{1,0:T(8,128)(2,1)S(1)}, bf16[256,1152]{1,0:T(8,128)(2,1)S(1)}, u32[]{:S(2)}, u32[]{:S(2)}) collective-permute-start(bf16[256,1152]{1,0:T(8,128)(2,1)S(1)} %collective-permute-done.4.m2), channel_id=1, source_target_pairs={{0,448},{1,57},{2,450},{3,59},{4,452},{5,61},{6,454},{7,63},{8,456... | collective-permute-start | bytes 1769480 | tf_op jit(solution)/shard_map/ppermute | solution.py:57
  50.7 4.4 %collective-permute-start.6 = (bf16[128,1152]{1,0:T(8,128)(2,1)S(1)}, bf16[128,1152]{1,0:T(8,128)(2,1)S(1)}, u32[]{:S(2)}, u32[]{:S(2)}) collective-permute-start(bf16[128,1152]{1,0:T(8,128)(2,1)S(1)} %slice.8), channel_id=1, source_target_pairs={{0,128},{1,17},{2,130},{3,19},{4,132},{5,21},{6,134},{7,23},{8,136... | collective-permute-start | bytes 884744 | tf_op jit(solution)/shard_map/ppermute | solution.py:57
  55.2 3.0 %collective-permute-start.7 = (bf16[128,1152]{1,0:T(8,128)(2,1)S(1)}, bf16[128,1152]{1,0:T(8,128)(2,1)S(1)}, u32[]{:S(2)}, u32[]{:S(2)}) collective-permute-start(bf16[128,1152]{1,0:T(8,128)(2,1)S(1)} %slice.9), channel_id=1, source_target_pairs={{0,384},{1,49},{2,386},{3,51},{4,388},{5,53},{6,390},{7,55},{8,392... | collective-permute-start | bytes 884744 | tf_op jit(solution)/shard_map/ppermute | solution.py:57
  60.4 2.6 %shard_map.79 = (bf16[2048,1152]{1,0:T(8,128)(2,1)S(1)}, f32[384,768]{1,0:T(8,128)S(1)}, f32[384,384]{1,0:T(8,128)S(1)}) custom-call(bf16[384,2048]{1,0:T(8,128)(2,1)S(1)} %get-tuple-element.15.norm_ref, bf16[384,2048]{1,0:T(8,128)(2,1)S(1)} %copy-done, bf16[256,1152]{1,0:T(8,128)(2,1)S(1)} %bitcast.10, bf16[256,1152]{1,0:T(8,128)(2,1)S(1)} %collective-permute-done.p1, ...), custom_call_target="tpu_custom_call" | custom-call | tf_op jit(solution)/shard_map/pallas_call | solution.py:185
  63.0 5.1 %collective-permute-done.7.m4 = bf16[128,1152]{1,0:T(8,128)(2,1)S(1)} collective-permute-done((bf16[128,1152]{1,0:T(8,128)(2,1)S(1)}, bf16[128,1152]{1,0:T(8,128)(2,1)S(1)}, u32[]{:S(2)}, u32[]{:S(2)}) %collective-permute-start.7) | collective-permute-done | bytes 294944 | tf_op jit(solution)/shard_map/ppermute | solution.py:57
  68.1 2.2 %shard_map.81 = (bf16[192,2048]{1,0:T(8,128)(2,1)S(1)}, bf16[192,2048]{1,0:T(8,128)(2,1)S(1)}, bf16[384,384]{1,0:T(8,128)(2,1)S(1)}, bf16[2048,1152]{1,0:T(8,128)(2,1)S(1)}) custom-call(bf16[2048,1152]{1,0:T(8,128)(2,1)S(1)} %get-tuple-element.16.w_in, f32[384,768]{1,0:T(8,128)S(1)} %get-tuple-element.17.gate_up_ref, ...), custom_call_target="tpu_custom_call", output_to_operand_aliasing={{3}: (0, {})} | custom-call | tf_op jit(solution)/shard_map/pallas_call | solution.py:200
  70.3 1.9 %shard_map.87 = bf16[2048,384]{1,0:T(8,128)(2,1)} custom-call(bf16[2048,384]{1,0:T(8,128)(2,1)S(1)} %get-tuple-element.20.turned_cot.turned_ref, bf16[384,384]{1,0:T(8,128)(2,1)S(1)} %get-tuple-element.25.hidden_ref), custom_call_target="tpu_custom_call" | custom-call | tf_op jit(solution)/shard_map/pallas_call | solution.py:236
  72.2 4.4 %all-to-all-start.1 = ((bf16[8,256,384]{2,1,0:T(8,128)(2,1)}), bf16[8,256,384]{2,1,0:T(8,128)(2,1)S(1)}, u32[]{:S(2)}, u32[]{:S(2)}) async-start(bf16[8,256,384]{2,1,0:T(8,128)(2,1)} %bitcast.3), calls=%async_computation.1 | async-start | bytes 3145728 | tf_op jit(solution)/shard_map/all_to_all | solution.py:61
  76.6 6.9 %collective-permute-start.8 = (bf16[192,2048]{1,0:T(8,128)(2,1)}, bf16[192,2048]{1,0:T(8,128)(2,1)S(1)}, u32[]{:S(2)}, u32[]{:S(2)}) collective-permute-start(bf16[192,2048]{1,0:T(8,128)(2,1)} %copy-done.3), channel_id=1, source_target_pairs={{0,1},{1,0},{2,3},{3,2},{4,5},{5,4},{6,7},{7,6},{8,9},{9,8},{10,11... | collective-permute-start | bytes 2359304 | tf_op jit(solution)/shard_map/ppermute | solution.py:316
  83.4 2.1 %collective-permute-done.8.right_ref = bf16[192,2048]{1,0:T(8,128)(2,1)S(1)} collective-permute-done((bf16[192,2048]{1,0:T(8,128)(2,1)}, bf16[192,2048]{1,0:T(8,128)(2,1)S(1)}, u32[]{:S(2)}, u32[]{:S(2)}) %collective-permute-start.8) | collective-permute-done | bytes 786464 | tf_op jit(solution)/shard_map/ppermute | solution.py:316
  85.7 4.4 %collective-permute-start.11 = (bf16[96,2048]{1,0:T(8,128)(2,1)S(1)}, bf16[96,2048]{1,0:T(8,128)(2,1)S(1)}, u32[]{:S(2)}, u32[]{:S(2)}) collective-permute-start(bf16[96,2048]{1,0:T(8,128)(2,1)S(1)} %get-tuple-element.24.left_ref), channel_id=1, source_target_pairs={{0,2},{1,7},{2,0},{3,5},{4,6},{5,3},{6,4},{7,1},{8,10},{9,15},{10,... | collective-permute-start | bytes 1179656 | tf_op jit(solution)/shard_map/ppermute | solution.py:312
  90.1 2.1 %collective-permute-start.9 = (bf16[96,2048]{1,0:T(8,128)(2,1)S(1)}, bf16[96,2048]{1,0:T(8,128)(2,1)S(1)}, u32[]{:S(2)}, u32[]{:S(2)}) collective-permute-start(bf16[96,2048]{1,0:T(8,128)(2,1)S(1)} %get-tuple-element.23.left_ref), channel_id=1, source_target_pairs={{0,2},{1,7},{2,0},{3,5},{4,6},{5,3},{6,4},{7,1},{8,10},{9,15},{10,... | collective-permute-start | bytes 1179656 | tf_op jit(solution)/shard_map/ppermute | solution.py:312
  92.2 3.5 %collective-permute-done.11.right_ref = bf16[96,2048]{1,0:T(8,128)(2,1)S(1)} collective-permute-done((bf16[96,2048]{1,0:T(8,128)(2,1)S(1)}, bf16[96,2048]{1,0:T(8,128)(2,1)S(1)}, u32[]{:S(2)}, u32[]{:S(2)}) %collective-permute-start.11) | collective-permute-done | bytes 393248 | tf_op jit(solution)/shard_map/ppermute | solution.py:312
  95.8 1.9 %collective-permute-start.12 = (bf16[96,2048]{1,0:T(8,128)(2,1)S(1)}, bf16[96,2048]{1,0:T(8,128)(2,1)S(1)}, u32[]{:S(2)}, u32[]{:S(2)}) collective-permute-start(bf16[96,2048]{1,0:T(8,128)(2,1)S(1)} %shard_map.84.left2), channel_id=1, source_target_pairs={{0,6},{1,3},{2,4},{3,1},{4,2},{5,7},{6,0},{7,5},{8,14},{9,11},{10,... | collective-permute-start | bytes 1179656 | tf_op jit(solution)/shard_map/ppermute | solution.py:312
  97.8 2.1 %collective-permute-done.9.right_ref = bf16[96,2048]{1,0:T(8,128)(2,1)S(1)} collective-permute-done((bf16[96,2048]{1,0:T(8,128)(2,1)S(1)}, bf16[96,2048]{1,0:T(8,128)(2,1)S(1)}, u32[]{:S(2)}, u32[]{:S(2)}) %collective-permute-start.9) | collective-permute-done | bytes 393248 | tf_op jit(solution)/shard_map/ppermute | solution.py:312
  99.9 2.0 %collective-permute-start.10 = (bf16[96,2048]{1,0:T(8,128)(2,1)S(1)}, bf16[96,2048]{1,0:T(8,128)(2,1)S(1)}, u32[]{:S(2)}, u32[]{:S(2)}) collective-permute-start(bf16[96,2048]{1,0:T(8,128)(2,1)S(1)} %shard_map.83.left1), channel_id=1, source_target_pairs={{0,6},{1,3},{2,4},{3,1},{4,2},{5,7},{6,0},{7,5},{8,14},{9,11},{10,... | collective-permute-start | bytes 1179656 | tf_op jit(solution)/shard_map/ppermute | solution.py:312
  102.2 2.4 %collective-permute-done.12.right2 = bf16[96,2048]{1,0:T(8,128)(2,1)S(1)} collective-permute-done((bf16[96,2048]{1,0:T(8,128)(2,1)S(1)}, bf16[96,2048]{1,0:T(8,128)(2,1)S(1)}, u32[]{:S(2)}, u32[]{:S(2)}) %collective-permute-start.12) | collective-permute-done | bytes 393248 | tf_op jit(solution)/shard_map/ppermute | solution.py:312
  104.7 4.2 %collective-permute-done.10.right1 = bf16[96,2048]{1,0:T(8,128)(2,1)S(1)} collective-permute-done((bf16[96,2048]{1,0:T(8,128)(2,1)S(1)}, bf16[96,2048]{1,0:T(8,128)(2,1)S(1)}, u32[]{:S(2)}, u32[]{:S(2)}) %collective-permute-start.10) | collective-permute-done | bytes 393248 | tf_op jit(solution)/shard_map/ppermute | solution.py:312
  109.7 4.6 %collective-permute-start.13 = (bf16[192,2048]{1,0:T(8,128)(2,1)S(1)}, bf16[192,2048]{1,0:T(8,128)(2,1)S(1)}, u32[]{:S(2)}, u32[]{:S(2)}) collective-permute-start(bf16[192,2048]{1,0:T(8,128)(2,1)S(1)} %shard_map.85.mine_ref), channel_id=1, source_target_pairs={{0,1},{1,0},{2,3},{3,2},{4,5},{5,4},{6,7},{7,6},{8,9},{9,8},{10,11... | collective-permute-start | bytes 2359304 | tf_op jit(solution)/shard_map/ppermute | solution.py:316
  114.3 0.9 shard_map.88
  115.2 6.9 %all-to-all-start.2 = ((bf16[8,32,384]{2,1,0:T(8,128)(2,1)}), bf16[8,32,384]{2,1,0:T(8,128)(2,1)S(1)}, u32[]{:S(2)}, u32[]{:S(2)}) async-start(bf16[8,32,384]{2,1,0:T(8,128)(2,1)} %bitcast.4), calls=%async_computation.2 | async-start | bytes 393216 | tf_op jit(solution)/shard_map/all_to_all | solution.py:61
  122.1 1.2 shard_map.86
  123.3 7.5 %all-to-all-done.2.parts_ref = bf16[8,32,384]{2,1,0:T(8,128)(2,1)S(1)} async-done(((bf16[8,32,384]{2,1,0:T(8,128)(2,1)}), bf16[8,32,384]{2,1,0:T(8,128)(2,1)S(1)}, u32[]{:S(2)}, u32[]{:S(2)}) %all-to-all-start.2) | async-done | bytes 196640 | tf_op jit(solution)/shard_map/all_to_all | solution.py:61
  (26 shorter events, 4.4 us)
Async XLA Ops:
  0.6 57.6 %copy-start.1 = (bf16[384,2048]{1,0:T(8,128)(2,1)S(1)}, bf16[384,2048]{1,0:T(8,128)(2,1)}, u32[]{:S(2)}) copy-start(bf16[384,2048]{1,0:T(8,128)(2,1)} %x_ref.1) | copy-start | bytes 4718596
  0.6 57.6 %copy-start.2 = (f32[2048]{0:T(1024)S(1)}, f32[2048]{0:T(1024)}, u32[]{:S(2)}) copy-start(f32[2048]{0:T(1024)} %param.7) | copy-start | bytes 24580
  25.1 33.8 %copy-start = (bf16[384,2048]{1,0:T(8,128)(2,1)S(1)}, bf16[384,2048]{1,0:T(8,128)(2,1)}, u32[]{:S(2)}) copy-start(bf16[384,2048]{1,0:T(8,128)(2,1)} %cot_ref.3) | copy-start | bytes 4718596
  25.1 16.5 %collective-permute-start.1 = (bf16[256,1152]{1,0:T(8,128)(2,1)S(1)}, bf16[256,1152]{1,0:T(8,128)(2,1)S(1)}, u32[]{:S(2)}, u32[]{:S(2)}) collective-permute-start(bf16[256,1152]{1,0:T(8,128)(2,1)S(1)} %bitcast.6), channel_id=1, source_target_pairs={{0,128},{1,17},{2,130},{3,19},{4,132},{5,21},{6,134},{7,23},{8,136... | collective-permute-start | bytes 1769480 | tf_op jit(solution)/shard_map/ppermute | solution.py:57
  29.4 19.4 %collective-permute-start.4 = (bf16[256,1152]{1,0:T(8,128)(2,1)S(1)}, bf16[256,1152]{1,0:T(8,128)(2,1)S(1)}, u32[]{:S(2)}, u32[]{:S(2)}) collective-permute-start(bf16[256,1152]{1,0:T(8,128)(2,1)S(1)} %bitcast.7), channel_id=1, source_target_pairs={{0,384},{1,49},{2,386},{3,51},{4,388},{5,53},{6,390},{7,55},{8,392... | collective-permute-start | bytes 1769480 | tf_op jit(solution)/shard_map/ppermute | solution.py:57
  33.0 22.1 %collective-permute-start = (bf16[256,1152]{1,0:T(8,128)(2,1)S(1)}, bf16[256,1152]{1,0:T(8,128)(2,1)S(1)}, u32[]{:S(2)}, u32[]{:S(2)}) collective-permute-start(bf16[256,1152]{1,0:T(8,128)(2,1)S(1)} %bitcast.8), channel_id=1, source_target_pairs={{0,64},{1,9},{2,66},{3,11},{4,68},{5,13},{6,70},{7,15},{8,72},{9,1... | collective-permute-start | bytes 1769480 | tf_op jit(solution)/shard_map/ppermute | solution.py:57
  35.8 23.9 %collective-permute-start.3 = (bf16[256,1152]{1,0:T(8,128)(2,1)S(1)}, bf16[256,1152]{1,0:T(8,128)(2,1)S(1)}, u32[]{:S(2)}, u32[]{:S(2)}) collective-permute-start(bf16[256,1152]{1,0:T(8,128)(2,1)S(1)} %bitcast.9), channel_id=1, source_target_pairs={{0,448},{1,57},{2,450},{3,59},{4,452},{5,61},{6,454},{7,63},{8,456... | collective-permute-start | bytes 1769480 | tf_op jit(solution)/shard_map/ppermute | solution.py:57
  41.6 18.1 %collective-permute-start.2 = (bf16[256,1152]{1,0:T(8,128)(2,1)S(1)}, bf16[256,1152]{1,0:T(8,128)(2,1)S(1)}, u32[]{:S(2)}, u32[]{:S(2)}) collective-permute-start(bf16[256,1152]{1,0:T(8,128)(2,1)S(1)} %collective-permute-done.1.p2), channel_id=1, source_target_pairs={{0,64},{1,9},{2,66},{3,11},{4,68},{5,13},{6,70},{7,15},{8,72},{9,1... | collective-permute-start | bytes 1769480 | tf_op jit(solution)/shard_map/ppermute | solution.py:57
  48.8 11.6 %collective-permute-start.5 = (bf16[256,1152]{1,0:T(8,128)(2,1)S(1)}, bf16[256,1152]{1,0:T(8,128)(2,1)S(1)}, u32[]{:S(2)}, u32[]{:S(2)}) collective-permute-start(bf16[256,1152]{1,0:T(8,128)(2,1)S(1)} %collective-permute-done.4.m2), channel_id=1, source_target_pairs={{0,448},{1,57},{2,450},{3,59},{4,452},{5,61},{6,454},{7,63},{8,456... | collective-permute-start | bytes 1769480 | tf_op jit(solution)/shard_map/ppermute | solution.py:57
  50.7 12.2 %collective-permute-start.6 = (bf16[128,1152]{1,0:T(8,128)(2,1)S(1)}, bf16[128,1152]{1,0:T(8,128)(2,1)S(1)}, u32[]{:S(2)}, u32[]{:S(2)}) collective-permute-start(bf16[128,1152]{1,0:T(8,128)(2,1)S(1)} %slice.8), channel_id=1, source_target_pairs={{0,128},{1,17},{2,130},{3,19},{4,132},{5,21},{6,134},{7,23},{8,136... | collective-permute-start | bytes 884744 | tf_op jit(solution)/shard_map/ppermute | solution.py:57
  55.2 12.9 %collective-permute-start.7 = (bf16[128,1152]{1,0:T(8,128)(2,1)S(1)}, bf16[128,1152]{1,0:T(8,128)(2,1)S(1)}, u32[]{:S(2)}, u32[]{:S(2)}) collective-permute-start(bf16[128,1152]{1,0:T(8,128)(2,1)S(1)} %slice.9), channel_id=1, source_target_pairs={{0,384},{1,49},{2,386},{3,51},{4,388},{5,53},{6,390},{7,55},{8,392... | collective-permute-start | bytes 884744 | tf_op jit(solution)/shard_map/ppermute | solution.py:57
  70.3 1.9 %copy-start.3 = (bf16[192,2048]{1,0:T(8,128)(2,1)}, bf16[192,2048]{1,0:T(8,128)(2,1)S(1)}, u32[]{:S(2)}) copy-start(bf16[192,2048]{1,0:T(8,128)(2,1)S(1)} %get-tuple-element.22) | copy-start | bytes 2359300
  72.2 42.1 %all-to-all-start.1 = ((bf16[8,256,384]{2,1,0:T(8,128)(2,1)}), bf16[8,256,384]{2,1,0:T(8,128)(2,1)S(1)}, u32[]{:S(2)}, u32[]{:S(2)}) async-start(bf16[8,256,384]{2,1,0:T(8,128)(2,1)} %bitcast.3), calls=%async_computation.1 | async-start | bytes 3145728 | tf_op jit(solution)/shard_map/all_to_all | solution.py:61
  76.6 9.0 %collective-permute-start.8 = (bf16[192,2048]{1,0:T(8,128)(2,1)}, bf16[192,2048]{1,0:T(8,128)(2,1)S(1)}, u32[]{:S(2)}, u32[]{:S(2)}) collective-permute-start(bf16[192,2048]{1,0:T(8,128)(2,1)} %copy-done.3), channel_id=1, source_target_pairs={{0,1},{1,0},{2,3},{3,2},{4,5},{5,4},{6,7},{7,6},{8,9},{9,8},{10,11... | collective-permute-start | bytes 2359304 | tf_op jit(solution)/shard_map/ppermute | solution.py:316
  85.7 10.0 %collective-permute-start.11 = (bf16[96,2048]{1,0:T(8,128)(2,1)S(1)}, bf16[96,2048]{1,0:T(8,128)(2,1)S(1)}, u32[]{:S(2)}, u32[]{:S(2)}) collective-permute-start(bf16[96,2048]{1,0:T(8,128)(2,1)S(1)} %get-tuple-element.24.left_ref), channel_id=1, source_target_pairs={{0,2},{1,7},{2,0},{3,5},{4,6},{5,3},{6,4},{7,1},{8,10},{9,15},{10,... | collective-permute-start | bytes 1179656 | tf_op jit(solution)/shard_map/ppermute | solution.py:312
  90.1 9.7 %collective-permute-start.9 = (bf16[96,2048]{1,0:T(8,128)(2,1)S(1)}, bf16[96,2048]{1,0:T(8,128)(2,1)S(1)}, u32[]{:S(2)}, u32[]{:S(2)}) collective-permute-start(bf16[96,2048]{1,0:T(8,128)(2,1)S(1)} %get-tuple-element.23.left_ref), channel_id=1, source_target_pairs={{0,2},{1,7},{2,0},{3,5},{4,6},{5,3},{6,4},{7,1},{8,10},{9,15},{10,... | collective-permute-start | bytes 1179656 | tf_op jit(solution)/shard_map/ppermute | solution.py:312
  95.8 8.8 %collective-permute-start.12 = (bf16[96,2048]{1,0:T(8,128)(2,1)S(1)}, bf16[96,2048]{1,0:T(8,128)(2,1)S(1)}, u32[]{:S(2)}, u32[]{:S(2)}) collective-permute-start(bf16[96,2048]{1,0:T(8,128)(2,1)S(1)} %shard_map.84.left2), channel_id=1, source_target_pairs={{0,6},{1,3},{2,4},{3,1},{4,2},{5,7},{6,0},{7,5},{8,14},{9,11},{10,... | collective-permute-start | bytes 1179656 | tf_op jit(solution)/shard_map/ppermute | solution.py:312
  99.9 8.9 %collective-permute-start.10 = (bf16[96,2048]{1,0:T(8,128)(2,1)S(1)}, bf16[96,2048]{1,0:T(8,128)(2,1)S(1)}, u32[]{:S(2)}, u32[]{:S(2)}) collective-permute-start(bf16[96,2048]{1,0:T(8,128)(2,1)S(1)} %shard_map.83.left1), channel_id=1, source_target_pairs={{0,6},{1,3},{2,4},{3,1},{4,2},{5,7},{6,0},{7,5},{8,14},{9,11},{10,... | collective-permute-start | bytes 1179656 | tf_op jit(solution)/shard_map/ppermute | solution.py:312
  109.7 12.4 %collective-permute-start.13 = (bf16[192,2048]{1,0:T(8,128)(2,1)S(1)}, bf16[192,2048]{1,0:T(8,128)(2,1)S(1)}, u32[]{:S(2)}, u32[]{:S(2)}) collective-permute-start(bf16[192,2048]{1,0:T(8,128)(2,1)S(1)} %shard_map.85.mine_ref), channel_id=1, source_target_pairs={{0,1},{1,0},{2,3},{3,2},{4,5},{5,4},{6,7},{7,6},{8,9},{9,8},{10,11... | collective-permute-start | bytes 2359304 | tf_op jit(solution)/shard_map/ppermute | solution.py:316
  115.2 15.6 %all-to-all-start.2 = ((bf16[8,32,384]{2,1,0:T(8,128)(2,1)}), bf16[8,32,384]{2,1,0:T(8,128)(2,1)S(1)}, u32[]{:S(2)}, u32[]{:S(2)}) async-start(bf16[8,32,384]{2,1,0:T(8,128)(2,1)} %bitcast.4), calls=%async_computation.2 | async-start | bytes 393216 | tf_op jit(solution)/shard_map/all_to_all | solution.py:61

commit v2 on v0

--- a/solution.py
+++ b/solution.py
@@ -248,15 +248,22 @@
         out[...] = total[k * rows : (k + 1) * rows].astype(jnp.bfloat16)
 
 
-def final_kernel(x_ref, gain_ref, left1, right1, left2, right2, out_ref):
+def inverse_kernel(x_ref, out_ref):
+    for k in range(4):
+        rows = pl.ds(k * QUARTER, QUARTER)
+        value = x_ref[rows, :].astype(jnp.float32)
+        inverse = lax.rsqrt(jnp.mean(value * value, axis=-1, keepdims=True) + EPSILON)
+        out_ref[rows, :] = jnp.broadcast_to(inverse, (QUARTER, 128))
+
+
+def final_kernel(x_ref, inverse_ref, gain_ref, left1, right1, left2, right2, out_ref):
     gain = gain_ref[...]
     for k in range(4):
         rows = pl.ds(k * QUARTER, QUARTER)
         part = pl.ds(k % 2 * QUARTER, QUARTER)
         left, right = ((left1, right1), (left2, right2))[k // 2]
-        value = x_ref[rows, :].astype(jnp.float32)
-        inverse = lax.rsqrt(jnp.mean(value * value, axis=-1, keepdims=True) + EPSILON)
-        normalized = value * inverse
+        inverse = inverse_ref[rows, :1]
+        normalized = x_ref[rows, :].astype(jnp.float32) * inverse
         total = left[part, :].astype(jnp.float32) + right[part, :].astype(jnp.float32)
         scaled = total * gain
         mean = jnp.mean(scaled * normalized, axis=-1, keepdims=True)
@@ -346,7 +353,10 @@
     far1 = with_partner(two1, False)
     (two2,) = small_call(pair_kernel, [piece], chip2, got2)
     far2 = with_partner(two2, False)
-    (mine,) = small_call(final_kernel, [half], x_half, row, two1, far1, two2, far2)
+    (inverse,) = small_call(
+        inverse_kernel, [jax.ShapeDtypeStruct((HALF, 128), jnp.float32)], x_half
+    )
+    (mine,) = small_call(final_kernel, [half], x_half, inverse, row, two1, far1, two2, far2)
     away = with_core(mine)
     whole = place(mine, away)
     return whole, grad_down

time: 134 us -> 132 us (0.985)
  starting transfers between devices: 64.7 us -> 62.8 us
    ppermute x2, starting transfers between devices: 13 us -> 11.4 us  [with_core(): return lax.ppermute(array, 'c', [(0, 1), (1, 0)])]
    pallas_call x7 -> x8, Pallas kernels: 3.33 us -> 3.44 us  [small_call(): pl.pallas_call(kernel, out_shape=tuple(out_shape), in_specs=vmem_specs(le...]
  transfers between devices with their start and end apart: 16 -> 16, of which waited for: 9 -> 10; matrix products, arithmetic and copies ran while one was open for 0% -> 0% of each run, Pallas kernels for 5% -> 6%
where the time goes in v2:
time: 132 us; the launch traced here: 131 us
  starting transfers between devices  62.8 us (48%)
  waiting for transfers between devices  30.8 us (23%)
  blocking collectives  23.5 us (18%)
  Pallas kernels  12.2 us (9%)
    ppermute x8, starting transfers between devices, ring(): return lax.ppermute(array, AXES, ring_pairs(step))  29.7 us
    all_to_all x1, blocking collectives, exchange(): lax.all_to_all(array, AXES, 0, 0, axis_index_groups=line_groups(along_rin...  23.5 us
    ppermute x4, waiting for transfers between devices, with_partner(): return lax.ppermute(array, AXES, pairs)  12.2 us
    ppermute x2, starting transfers between devices, with_core(): return lax.ppermute(array, 'c', [(0, 1), (1, 0)])  11.4 us
    all_to_all x2, starting transfers between devices, exchange(): lax.all_to_all(array, AXES, 0, 0, axis_index_groups=line_groups(along_rin...  11.3 us
    ppermute x4, starting transfers between devices, with_partner(): return lax.ppermute(array, AXES, pairs)  10.4 us
    ppermute x8, waiting for transfers between devices, ring(): return lax.ppermute(array, AXES, ring_pairs(step))  9.02 us
    all_to_all x2, waiting for transfers between devices, exchange(): lax.all_to_all(array, AXES, 0, 0, axis_index_groups=line_groups(along_rin...  7.46 us
  transfers between devices with their start and end apart: 16, of which 10 were waited for; matrix products, arithmetic and copies ran while one was open for 0% of the time, Pallas kernels for 6%

profile of v2, /device:TPU:1, one launch (start us, length us, event | category | flops | bytes accessed | tf_op | source)
XLA Modules:
  0.0 131.2 jit_solution(6597151734929225520)
XLA Ops:
  0.7 0.9 fusion.5
  1.6 23.5 %all_to_all.15 = bf16[8,32,1152]{2,1,0:T(8,128)(2,1)S(1)} all-to-all(bf16[8,32,1152]{2,1,0:T(8,128)(2,1)S(1)} %broadcast_in_dim.2), channel_id=1, replica_groups={{0,8,16,24,32,40,48,56},{64,72,80,88,96,104,112,120},{128,136,144,152,1..., dimensions={0} | all-to-all | bytes 1179648 | tf_op jit(solution)/shard_map/all_to_all | solution.py:62
  25.1 4.3 %collective-permute-start.1 = (bf16[256,1152]{1,0:T(8,128)(2,1)S(1)}, bf16[256,1152]{1,0:T(8,128)(2,1)S(1)}, u32[]{:S(2)}, u32[]{:S(2)}) collective-permute-start(bf16[256,1152]{1,0:T(8,128)(2,1)S(1)} %bitcast.6), channel_id=1, source_target_pairs={{0,128},{1,17},{2,130},{3,19},{4,132},{5,21},{6,134},{7,23},{8,136... | collective-permute-start | bytes 1769480 | tf_op jit(solution)/shard_map/ppermute | solution.py:58
  29.4 3.6 %collective-permute-start.4 = (bf16[256,1152]{1,0:T(8,128)(2,1)S(1)}, bf16[256,1152]{1,0:T(8,128)(2,1)S(1)}, u32[]{:S(2)}, u32[]{:S(2)}) collective-permute-start(bf16[256,1152]{1,0:T(8,128)(2,1)S(1)} %bitcast.7), channel_id=1, source_target_pairs={{0,384},{1,49},{2,386},{3,51},{4,388},{5,53},{6,390},{7,55},{8,392... | collective-permute-start | bytes 1769480 | tf_op jit(solution)/shard_map/ppermute | solution.py:58
  33.0 2.8 %collective-permute-start = (bf16[256,1152]{1,0:T(8,128)(2,1)S(1)}, bf16[256,1152]{1,0:T(8,128)(2,1)S(1)}, u32[]{:S(2)}, u32[]{:S(2)}) collective-permute-start(bf16[256,1152]{1,0:T(8,128)(2,1)S(1)} %bitcast.8), channel_id=1, source_target_pairs={{0,64},{1,9},{2,66},{3,11},{4,68},{5,13},{6,70},{7,15},{8,72},{9,1... | collective-permute-start | bytes 1769480 | tf_op jit(solution)/shard_map/ppermute | solution.py:58
  35.8 3.7 %collective-permute-start.3 = (bf16[256,1152]{1,0:T(8,128)(2,1)S(1)}, bf16[256,1152]{1,0:T(8,128)(2,1)S(1)}, u32[]{:S(2)}, u32[]{:S(2)}) collective-permute-start(bf16[256,1152]{1,0:T(8,128)(2,1)S(1)} %bitcast.9), channel_id=1, source_target_pairs={{0,448},{1,57},{2,450},{3,59},{4,452},{5,61},{6,454},{7,63},{8,456... | collective-permute-start | bytes 1769480 | tf_op jit(solution)/shard_map/ppermute | solution.py:58
  39.5 2.1 %collective-permute-done.1.p2 = bf16[256,1152]{1,0:T(8,128)(2,1)S(1)} collective-permute-done((bf16[256,1152]{1,0:T(8,128)(2,1)S(1)}, bf16[256,1152]{1,0:T(8,128)(2,1)S(1)}, u32[]{:S(2)}, u32[]{:S(2)}) %collective-permute-start.1) | collective-permute-done | bytes 589856 | tf_op jit(solution)/shard_map/ppermute | solution.py:58
  41.6 5.9 %collective-permute-start.2 = (bf16[256,1152]{1,0:T(8,128)(2,1)S(1)}, bf16[256,1152]{1,0:T(8,128)(2,1)S(1)}, u32[]{:S(2)}, u32[]{:S(2)}) collective-permute-start(bf16[256,1152]{1,0:T(8,128)(2,1)S(1)} %collective-permute-done.1.p2), channel_id=1, source_target_pairs={{0,64},{1,9},{2,66},{3,11},{4,68},{5,13},{6,70},{7,15},{8,72},{9,1... | collective-permute-start | bytes 1769480 | tf_op jit(solution)/shard_map/ppermute | solution.py:58
  47.6 1.2 collective-permute-done.4.m2
  48.8 1.9 %collective-permute-start.5 = (bf16[256,1152]{1,0:T(8,128)(2,1)S(1)}, bf16[256,1152]{1,0:T(8,128)(2,1)S(1)}, u32[]{:S(2)}, u32[]{:S(2)}) collective-permute-start(bf16[256,1152]{1,0:T(8,128)(2,1)S(1)} %collective-permute-done.4.m2), channel_id=1, source_target_pairs={{0,448},{1,57},{2,450},{3,59},{4,452},{5,61},{6,454},{7,63},{8,456... | collective-permute-start | bytes 1769480 | tf_op jit(solution)/shard_map/ppermute | solution.py:58
  50.7 4.4 %collective-permute-start.6 = (bf16[128,1152]{1,0:T(8,128)(2,1)S(1)}, bf16[128,1152]{1,0:T(8,128)(2,1)S(1)}, u32[]{:S(2)}, u32[]{:S(2)}) collective-permute-start(bf16[128,1152]{1,0:T(8,128)(2,1)S(1)} %slice.8), channel_id=1, source_target_pairs={{0,128},{1,17},{2,130},{3,19},{4,132},{5,21},{6,134},{7,23},{8,136... | collective-permute-start | bytes 884744 | tf_op jit(solution)/shard_map/ppermute | solution.py:58
  55.2 3.0 %collective-permute-start.7 = (bf16[128,1152]{1,0:T(8,128)(2,1)S(1)}, bf16[128,1152]{1,0:T(8,128)(2,1)S(1)}, u32[]{:S(2)}, u32[]{:S(2)}) collective-permute-start(bf16[128,1152]{1,0:T(8,128)(2,1)S(1)} %slice.9), channel_id=1, source_target_pairs={{0,384},{1,49},{2,386},{3,51},{4,388},{5,53},{6,390},{7,55},{8,392... | collective-permute-start | bytes 884744 | tf_op jit(solution)/shard_map/ppermute | solution.py:58
  60.4 2.6 %shard_map.79 = (bf16[2048,1152]{1,0:T(8,128)(2,1)S(1)}, f32[384,768]{1,0:T(8,128)S(1)}, f32[384,384]{1,0:T(8,128)S(1)}) custom-call(bf16[384,2048]{1,0:T(8,128)(2,1)S(1)} %get-tuple-element.15.norm_ref, bf16[384,2048]{1,0:T(8,128)(2,1)S(1)} %copy-done, bf16[256,1152]{1,0:T(8,128)(2,1)S(1)} %bitcast.10, bf16[256,1152]{1,0:T(8,128)(2,1)S(1)} %collective-permute-done.p1, ...), custom_call_target="tpu_custom_call" | custom-call | tf_op jit(solution)/shard_map/pallas_call | solution.py:185
  63.0 5.1 %collective-permute-done.7.m4 = bf16[128,1152]{1,0:T(8,128)(2,1)S(1)} collective-permute-done((bf16[128,1152]{1,0:T(8,128)(2,1)S(1)}, bf16[128,1152]{1,0:T(8,128)(2,1)S(1)}, u32[]{:S(2)}, u32[]{:S(2)}) %collective-permute-start.7) | collective-permute-done | bytes 294944 | tf_op jit(solution)/shard_map/ppermute | solution.py:58
  68.1 2.3 %shard_map.81 = (bf16[192,2048]{1,0:T(8,128)(2,1)S(1)}, bf16[192,2048]{1,0:T(8,128)(2,1)S(1)}, bf16[384,384]{1,0:T(8,128)(2,1)S(1)}, bf16[2048,1152]{1,0:T(8,128)(2,1)S(1)}) custom-call(bf16[2048,1152]{1,0:T(8,128)(2,1)S(1)} %get-tuple-element.16.w_in, f32[384,768]{1,0:T(8,128)S(1)} %get-tuple-element.17.gate_up_ref, ...), custom_call_target="tpu_custom_call", output_to_operand_aliasing={{3}: (0, {})} | custom-call | tf_op jit(solution)/shard_map/pallas_call | solution.py:200
  70.3 1.9 %shard_map.87 = bf16[2048,384]{1,0:T(8,128)(2,1)} custom-call(bf16[2048,384]{1,0:T(8,128)(2,1)S(1)} %get-tuple-element.20.turned_cot.turned_ref, bf16[384,384]{1,0:T(8,128)(2,1)S(1)} %get-tuple-element.25.hidden_ref), custom_call_target="tpu_custom_call" | custom-call | tf_op jit(solution)/shard_map/pallas_call | solution.py:234
  72.2 4.4 %all-to-all-start.1 = ((bf16[8,256,384]{2,1,0:T(8,128)(2,1)}), bf16[8,256,384]{2,1,0:T(8,128)(2,1)S(1)}, u32[]{:S(2)}, u32[]{:S(2)}) async-start(bf16[8,256,384]{2,1,0:T(8,128)(2,1)} %bitcast.3), calls=%async_computation.1 | async-start | bytes 3145728 | tf_op jit(solution)/shard_map/all_to_all | solution.py:62
  76.6 6.8 %collective-permute-start.8 = (bf16[192,2048]{1,0:T(8,128)(2,1)}, bf16[192,2048]{1,0:T(8,128)(2,1)S(1)}, u32[]{:S(2)}, u32[]{:S(2)}) collective-permute-start(bf16[192,2048]{1,0:T(8,128)(2,1)} %copy-done.3), channel_id=1, source_target_pairs={{0,1},{1,0},{2,3},{3,2},{4,5},{5,4},{6,7},{7,6},{8,9},{9,8},{10,11... | collective-permute-start | bytes 2359304 | tf_op jit(solution)/shard_map/ppermute | solution.py:315
  83.4 2.1 %collective-permute-done.8.right_ref = bf16[192,2048]{1,0:T(8,128)(2,1)S(1)} collective-permute-done((bf16[192,2048]{1,0:T(8,128)(2,1)}, bf16[192,2048]{1,0:T(8,128)(2,1)S(1)}, u32[]{:S(2)}, u32[]{:S(2)}) %collective-permute-start.8) | collective-permute-done | bytes 786464 | tf_op jit(solution)/shard_map/ppermute | solution.py:315
  85.7 4.4 %collective-permute-start.11 = (bf16[96,2048]{1,0:T(8,128)(2,1)S(1)}, bf16[96,2048]{1,0:T(8,128)(2,1)S(1)}, u32[]{:S(2)}, u32[]{:S(2)}) collective-permute-start(bf16[96,2048]{1,0:T(8,128)(2,1)S(1)} %get-tuple-element.24.left_ref), channel_id=1, source_target_pairs={{0,2},{1,7},{2,0},{3,5},{4,6},{5,3},{6,4},{7,1},{8,10},{9,15},{10,... | collective-permute-start | bytes 1179656 | tf_op jit(solution)/shard_map/ppermute | solution.py:311
  90.1 2.1 %collective-permute-start.9 = (bf16[96,2048]{1,0:T(8,128)(2,1)S(1)}, bf16[96,2048]{1,0:T(8,128)(2,1)S(1)}, u32[]{:S(2)}, u32[]{:S(2)}) collective-permute-start(bf16[96,2048]{1,0:T(8,128)(2,1)S(1)} %get-tuple-element.23.left_ref), channel_id=1, source_target_pairs={{0,2},{1,7},{2,0},{3,5},{4,6},{5,3},{6,4},{7,1},{8,10},{9,15},{10,... | collective-permute-start | bytes 1179656 | tf_op jit(solution)/shard_map/ppermute | solution.py:311
  92.2 3.5 %collective-permute-done.11.right_ref = bf16[96,2048]{1,0:T(8,128)(2,1)S(1)} collective-permute-done((bf16[96,2048]{1,0:T(8,128)(2,1)S(1)}, bf16[96,2048]{1,0:T(8,128)(2,1)S(1)}, u32[]{:S(2)}, u32[]{:S(2)}) %collective-permute-start.11) | collective-permute-done | bytes 393248 | tf_op jit(solution)/shard_map/ppermute | solution.py:311
  95.8 1.9 %collective-permute-start.12 = (bf16[96,2048]{1,0:T(8,128)(2,1)S(1)}, bf16[96,2048]{1,0:T(8,128)(2,1)S(1)}, u32[]{:S(2)}, u32[]{:S(2)}) collective-permute-start(bf16[96,2048]{1,0:T(8,128)(2,1)S(1)} %shard_map.84.left2), channel_id=1, source_target_pairs={{0,6},{1,3},{2,4},{3,1},{4,2},{5,7},{6,0},{7,5},{8,14},{9,11},{10,... | collective-permute-start | bytes 1179656 | tf_op jit(solution)/shard_map/ppermute | solution.py:311
  97.8 2.1 %collective-permute-done.9.right_ref = bf16[96,2048]{1,0:T(8,128)(2,1)S(1)} collective-permute-done((bf16[96,2048]{1,0:T(8,128)(2,1)S(1)}, bf16[96,2048]{1,0:T(8,128)(2,1)S(1)}, u32[]{:S(2)}, u32[]{:S(2)}) %collective-permute-start.9) | collective-permute-done | bytes 393248 | tf_op jit(solution)/shard_map/ppermute | solution.py:311
  99.9 2.0 %collective-permute-start.10 = (bf16[96,2048]{1,0:T(8,128)(2,1)S(1)}, bf16[96,2048]{1,0:T(8,128)(2,1)S(1)}, u32[]{:S(2)}, u32[]{:S(2)}) collective-permute-start(bf16[96,2048]{1,0:T(8,128)(2,1)S(1)} %shard_map.83.left1), channel_id=1, source_target_pairs={{0,6},{1,3},{2,4},{3,1},{4,2},{5,7},{6,0},{7,5},{8,14},{9,11},{10,... | collective-permute-start | bytes 1179656 | tf_op jit(solution)/shard_map/ppermute | solution.py:311
  102.2 2.5 %collective-permute-done.12.right2 = bf16[96,2048]{1,0:T(8,128)(2,1)S(1)} collective-permute-done((bf16[96,2048]{1,0:T(8,128)(2,1)S(1)}, bf16[96,2048]{1,0:T(8,128)(2,1)S(1)}, u32[]{:S(2)}, u32[]{:S(2)}) %collective-permute-start.12) | collective-permute-done | bytes 393248 | tf_op jit(solution)/shard_map/ppermute | solution.py:311
  104.7 4.2 %collective-permute-done.10.right1 = bf16[96,2048]{1,0:T(8,128)(2,1)S(1)} collective-permute-done((bf16[96,2048]{1,0:T(8,128)(2,1)S(1)}, bf16[96,2048]{1,0:T(8,128)(2,1)S(1)}, u32[]{:S(2)}, u32[]{:S(2)}) %collective-permute-start.10) | collective-permute-done | bytes 393248 | tf_op jit(solution)/shard_map/ppermute | solution.py:311
  109.5 4.5 %collective-permute-start.13 = (bf16[192,2048]{1,0:T(8,128)(2,1)S(1)}, bf16[192,2048]{1,0:T(8,128)(2,1)S(1)}, u32[]{:S(2)}, u32[]{:S(2)}) collective-permute-start(bf16[192,2048]{1,0:T(8,128)(2,1)S(1)} %shard_map.85.mine_ref), channel_id=1, source_target_pairs={{0,1},{1,0},{2,3},{3,2},{4,5},{5,4},{6,7},{7,6},{8,9},{9,8},{10,11... | collective-permute-start | bytes 2359304 | tf_op jit(solution)/shard_map/ppermute | solution.py:315
  114.1 0.9 shard_map.88
  115.0 6.9 %all-to-all-start.2 = ((bf16[8,32,384]{2,1,0:T(8,128)(2,1)}), bf16[8,32,384]{2,1,0:T(8,128)(2,1)S(1)}, u32[]{:S(2)}, u32[]{:S(2)}) async-start(bf16[8,32,384]{2,1,0:T(8,128)(2,1)} %bitcast.4), calls=%async_computation.2 | async-start | bytes 393216 | tf_op jit(solution)/shard_map/all_to_all | solution.py:62
  121.9 1.2 shard_map.86
  123.1 7.5 %all-to-all-done.2.parts_ref = bf16[8,32,384]{2,1,0:T(8,128)(2,1)S(1)} async-done(((bf16[8,32,384]{2,1,0:T(8,128)(2,1)}), bf16[8,32,384]{2,1,0:T(8,128)(2,1)S(1)}, u32[]{:S(2)}, u32[]{:S(2)}) %all-to-all-start.2) | async-done | bytes 196640 | tf_op jit(solution)/shard_map/all_to_all | solution.py:62
  (26 shorter events, 4.2 us)
Async XLA Ops:
  0.6 57.6 %copy-start.1 = (bf16[384,2048]{1,0:T(8,128)(2,1)S(1)}, bf16[384,2048]{1,0:T(8,128)(2,1)}, u32[]{:S(2)}) copy-start(bf16[384,2048]{1,0:T(8,128)(2,1)} %x_ref.1) | copy-start | bytes 4718596
  0.6 57.6 %copy-start.2 = (f32[2048]{0:T(1024)S(1)}, f32[2048]{0:T(1024)}, u32[]{:S(2)}) copy-start(f32[2048]{0:T(1024)} %param.7) | copy-start | bytes 24580
  25.1 33.8 %copy-start = (bf16[384,2048]{1,0:T(8,128)(2,1)S(1)}, bf16[384,2048]{1,0:T(8,128)(2,1)}, u32[]{:S(2)}) copy-start(bf16[384,2048]{1,0:T(8,128)(2,1)} %cot_ref.3) | copy-start | bytes 4718596
  25.1 16.5 %collective-permute-start.1 = (bf16[256,1152]{1,0:T(8,128)(2,1)S(1)}, bf16[256,1152]{1,0:T(8,128)(2,1)S(1)}, u32[]{:S(2)}, u32[]{:S(2)}) collective-permute-start(bf16[256,1152]{1,0:T(8,128)(2,1)S(1)} %bitcast.6), channel_id=1, source_target_pairs={{0,128},{1,17},{2,130},{3,19},{4,132},{5,21},{6,134},{7,23},{8,136... | collective-permute-start | bytes 1769480 | tf_op jit(solution)/shard_map/ppermute | solution.py:58
  29.4 19.4 %collective-permute-start.4 = (bf16[256,1152]{1,0:T(8,128)(2,1)S(1)}, bf16[256,1152]{1,0:T(8,128)(2,1)S(1)}, u32[]{:S(2)}, u32[]{:S(2)}) collective-permute-start(bf16[256,1152]{1,0:T(8,128)(2,1)S(1)} %bitcast.7), channel_id=1, source_target_pairs={{0,384},{1,49},{2,386},{3,51},{4,388},{5,53},{6,390},{7,55},{8,392... | collective-permute-start | bytes 1769480 | tf_op jit(solution)/shard_map/ppermute | solution.py:58
  33.0 22.1 %collective-permute-start = (bf16[256,1152]{1,0:T(8,128)(2,1)S(1)}, bf16[256,1152]{1,0:T(8,128)(2,1)S(1)}, u32[]{:S(2)}, u32[]{:S(2)}) collective-permute-start(bf16[256,1152]{1,0:T(8,128)(2,1)S(1)} %bitcast.8), channel_id=1, source_target_pairs={{0,64},{1,9},{2,66},{3,11},{4,68},{5,13},{6,70},{7,15},{8,72},{9,1... | collective-permute-start | bytes 1769480 | tf_op jit(solution)/shard_map/ppermute | solution.py:58
  35.8 23.9 %collective-permute-start.3 = (bf16[256,1152]{1,0:T(8,128)(2,1)S(1)}, bf16[256,1152]{1,0:T(8,128)(2,1)S(1)}, u32[]{:S(2)}, u32[]{:S(2)}) collective-permute-start(bf16[256,1152]{1,0:T(8,128)(2,1)S(1)} %bitcast.9), channel_id=1, source_target_pairs={{0,448},{1,57},{2,450},{3,59},{4,452},{5,61},{6,454},{7,63},{8,456... | collective-permute-start | bytes 1769480 | tf_op jit(solution)/shard_map/ppermute | solution.py:58
  41.6 18.1 %collective-permute-start.2 = (bf16[256,1152]{1,0:T(8,128)(2,1)S(1)}, bf16[256,1152]{1,0:T(8,128)(2,1)S(1)}, u32[]{:S(2)}, u32[]{:S(2)}) collective-permute-start(bf16[256,1152]{1,0:T(8,128)(2,1)S(1)} %collective-permute-done.1.p2), channel_id=1, source_target_pairs={{0,64},{1,9},{2,66},{3,11},{4,68},{5,13},{6,70},{7,15},{8,72},{9,1... | collective-permute-start | bytes 1769480 | tf_op jit(solution)/shard_map/ppermute | solution.py:58
  48.8 11.6 %collective-permute-start.5 = (bf16[256,1152]{1,0:T(8,128)(2,1)S(1)}, bf16[256,1152]{1,0:T(8,128)(2,1)S(1)}, u32[]{:S(2)}, u32[]{:S(2)}) collective-permute-start(bf16[256,1152]{1,0:T(8,128)(2,1)S(1)} %collective-permute-done.4.m2), channel_id=1, source_target_pairs={{0,448},{1,57},{2,450},{3,59},{4,452},{5,61},{6,454},{7,63},{8,456... | collective-permute-start | bytes 1769480 | tf_op jit(solution)/shard_map/ppermute | solution.py:58
  50.7 12.2 %collective-permute-start.6 = (bf16[128,1152]{1,0:T(8,128)(2,1)S(1)}, bf16[128,1152]{1,0:T(8,128)(2,1)S(1)}, u32[]{:S(2)}, u32[]{:S(2)}) collective-permute-start(bf16[128,1152]{1,0:T(8,128)(2,1)S(1)} %slice.8), channel_id=1, source_target_pairs={{0,128},{1,17},{2,130},{3,19},{4,132},{5,21},{6,134},{7,23},{8,136... | collective-permute-start | bytes 884744 | tf_op jit(solution)/shard_map/ppermute | solution.py:58
  55.2 12.9 %collective-permute-start.7 = (bf16[128,1152]{1,0:T(8,128)(2,1)S(1)}, bf16[128,1152]{1,0:T(8,128)(2,1)S(1)}, u32[]{:S(2)}, u32[]{:S(2)}) collective-permute-start(bf16[128,1152]{1,0:T(8,128)(2,1)S(1)} %slice.9), channel_id=1, source_target_pairs={{0,384},{1,49},{2,386},{3,51},{4,388},{5,53},{6,390},{7,55},{8,392... | collective-permute-start | bytes 884744 | tf_op jit(solution)/shard_map/ppermute | solution.py:58
  70.3 1.9 %copy-start.3 = (bf16[192,2048]{1,0:T(8,128)(2,1)}, bf16[192,2048]{1,0:T(8,128)(2,1)S(1)}, u32[]{:S(2)}) copy-start(bf16[192,2048]{1,0:T(8,128)(2,1)S(1)} %get-tuple-element.22) | copy-start | bytes 2359300
  72.2 41.9 %all-to-all-start.1 = ((bf16[8,256,384]{2,1,0:T(8,128)(2,1)}), bf16[8,256,384]{2,1,0:T(8,128)(2,1)S(1)}, u32[]{:S(2)}, u32[]{:S(2)}) async-start(bf16[8,256,384]{2,1,0:T(8,128)(2,1)} %bitcast.3), calls=%async_computation.1 | async-start | bytes 3145728 | tf_op jit(solution)/shard_map/all_to_all | solution.py:62
  76.6 8.9 %collective-permute-start.8 = (bf16[192,2048]{1,0:T(8,128)(2,1)}, bf16[192,2048]{1,0:T(8,128)(2,1)S(1)}, u32[]{:S(2)}, u32[]{:S(2)}) collective-permute-start(bf16[192,2048]{1,0:T(8,128)(2,1)} %copy-done.3), channel_id=1, source_target_pairs={{0,1},{1,0},{2,3},{3,2},{4,5},{5,4},{6,7},{7,6},{8,9},{9,8},{10,11... | collective-permute-start | bytes 2359304 | tf_op jit(solution)/shard_map/ppermute | solution.py:315
  85.7 10.0 %collective-permute-start.11 = (bf16[96,2048]{1,0:T(8,128)(2,1)S(1)}, bf16[96,2048]{1,0:T(8,128)(2,1)S(1)}, u32[]{:S(2)}, u32[]{:S(2)}) collective-permute-start(bf16[96,2048]{1,0:T(8,128)(2,1)S(1)} %get-tuple-element.24.left_ref), channel_id=1, source_target_pairs={{0,2},{1,7},{2,0},{3,5},{4,6},{5,3},{6,4},{7,1},{8,10},{9,15},{10,... | collective-permute-start | bytes 1179656 | tf_op jit(solution)/shard_map/ppermute | solution.py:311
  90.1 9.7 %collective-permute-start.9 = (bf16[96,2048]{1,0:T(8,128)(2,1)S(1)}, bf16[96,2048]{1,0:T(8,128)(2,1)S(1)}, u32[]{:S(2)}, u32[]{:S(2)}) collective-permute-start(bf16[96,2048]{1,0:T(8,128)(2,1)S(1)} %get-tuple-element.23.left_ref), channel_id=1, source_target_pairs={{0,2},{1,7},{2,0},{3,5},{4,6},{5,3},{6,4},{7,1},{8,10},{9,15},{10,... | collective-permute-start | bytes 1179656 | tf_op jit(solution)/shard_map/ppermute | solution.py:311
  95.8 8.8 %collective-permute-start.12 = (bf16[96,2048]{1,0:T(8,128)(2,1)S(1)}, bf16[96,2048]{1,0:T(8,128)(2,1)S(1)}, u32[]{:S(2)}, u32[]{:S(2)}) collective-permute-start(bf16[96,2048]{1,0:T(8,128)(2,1)S(1)} %shard_map.84.left2), channel_id=1, source_target_pairs={{0,6},{1,3},{2,4},{3,1},{4,2},{5,7},{6,0},{7,5},{8,14},{9,11},{10,... | collective-permute-start | bytes 1179656 | tf_op jit(solution)/shard_map/ppermute | solution.py:311
  99.9 8.9 %collective-permute-start.10 = (bf16[96,2048]{1,0:T(8,128)(2,1)S(1)}, bf16[96,2048]{1,0:T(8,128)(2,1)S(1)}, u32[]{:S(2)}, u32[]{:S(2)}) collective-permute-start(bf16[96,2048]{1,0:T(8,128)(2,1)S(1)} %shard_map.83.left1), channel_id=1, source_target_pairs={{0,6},{1,3},{2,4},{3,1},{4,2},{5,7},{6,0},{7,5},{8,14},{9,11},{10,... | collective-permute-start | bytes 1179656 | tf_op jit(solution)/shard_map/ppermute | solution.py:311
  109.5 12.4 %collective-permute-start.13 = (bf16[192,2048]{1,0:T(8,128)(2,1)S(1)}, bf16[192,2048]{1,0:T(8,128)(2,1)S(1)}, u32[]{:S(2)}, u32[]{:S(2)}) collective-permute-start(bf16[192,2048]{1,0:T(8,128)(2,1)S(1)} %shard_map.85.mine_ref), channel_id=1, source_target_pairs={{0,1},{1,0},{2,3},{3,2},{4,5},{5,4},{6,7},{7,6},{8,9},{9,8},{10,11... | collective-permute-start | bytes 2359304 | tf_op jit(solution)/shard_map/ppermute | solution.py:315
  115.0 15.6 %all-to-all-start.2 = ((bf16[8,32,384]{2,1,0:T(8,128)(2,1)}), bf16[8,32,384]{2,1,0:T(8,128)(2,1)S(1)}, u32[]{:S(2)}, u32[]{:S(2)}) async-start(bf16[8,32,384]{2,1,0:T(8,128)(2,1)} %bitcast.4), calls=%async_computation.2 | async-start | bytes 393216 | tf_op jit(solution)/shard_map/all_to_all | solution.py:62
